TPU v7x, 32 devices: a whole 2x2x4 slice. The times are simulated.
32 devices in a mesh: rep: 2 (over x), fs: 8 (over z, y), tp: 2 (over core).
Axes of the slice: x: 2, y: 2, z: 4, core: 2. Of those that a mesh axis runs over, the one named last changes fastest.
Arguments:
- tokens: bfloat16 [16, 64, 2048], P(('rep', 'fs'), None, 'tp'), may hold values from -6 to 6
- lin_weight: bfloat16 [2048, 1024], P('fs', 'tp'), may hold values from -0.125 to 0.125
- glu_weight: bfloat16 [2048, 1024], P('fs', 'tp'), may hold values from -0.125 to 0.125
- conv_taps: float32 [31, 1024], P(None, 'tp'), may hold values from -4 to 4
- conv_gain: float32 [1024], P('tp'), may hold values from 0.1 to 1.9
- conv_out_weight: bfloat16 [1024, 2048], P('tp', 'fs'), may hold values from -0.1875 to 0.1875
- mix_gain: float32 [2048], replicated, may hold values from 0.1 to 1.9
- ff_gate: bfloat16 [2048, 5632], P('fs', 'tp'), may hold values from -0.125 to 0.125
- ff_up: bfloat16 [2048, 5632], P('fs', 'tp'), may hold values from -0.125 to 0.125
- ff_down: bfloat16 [5632, 2048], P('tp', 'fs'), may hold values from -0.078125 to 0.078125
- out_gain: float32 [2048], replicated, may hold values from 0.1 to 1.9
Outputs:
- encoded: bfloat16 [16, 64, 2048], P(('rep', 'fs'), None, 'tp')
All inputs are finite; a program needn't handle non-finite values.
Results may differ from a plain program's by a relative error of at most 0.014.
Values may be sent and summed in bfloat16 or wider, within the bound.
A program may use at most 128 MiB of HBM per device.

v0:
```python
import functools

import jax
import jax.numpy as jnp
from jax import lax
from jax.experimental import pallas as pl
from jax.experimental.pallas import tpu as pltpu
from jax.sharding import PartitionSpec as P

residual_scale = 2.0**0.25
epsilon = 1e-05


def normed(values):
    average = jnp.mean(values, axis=-1, keepdims=True)
    second = jnp.mean(values * values, axis=-1, keepdims=True)
    return (values - average) * lax.rsqrt(second - average * average + epsilon)


def interleave(left, right, parts):
    rows, width = left.shape
    pair = jnp.concatenate(
        (left.reshape(rows, parts, width // parts), right.reshape(rows, parts, width // parts)),
        axis=2,
    )
    return pair.reshape(rows, 2 * width)


def by_collectives(
    tokens,
    lin_weight,
    glu_weight,
    conv_taps,
    conv_gain,
    conv_out_weight,
    mix_gain,
    ff_gate,
    ff_up,
    ff_down,
    out_gain,
):
    n_fs, n_tp = lax.axis_size("fs"), lax.axis_size("tp")
    fs_index, tp_index = lax.axis_index("fs"), lax.axis_index("tp")
    seqs, length, feat = tokens.shape
    groups = n_fs * seqs
    rows = groups * length
    model = feat * n_tp
    conv_gain_all = lax.all_gather(conv_gain, "tp", axis=0, tiled=True)

    gathered = lax.all_gather(tokens, ("fs", "tp"), axis=0, tiled=False)
    all_tokens = (
        gathered.reshape(n_fs, n_tp, seqs, length, feat)
        .transpose(0, 2, 3, 1, 4)
        .reshape(rows, model)
    )
    glu_pair = lax.all_to_all(
        interleave(lin_weight, glu_weight, n_fs), "fs", split_axis=1, concat_axis=0, tiled=True
    )
    own_out = lax.all_to_all(conv_out_weight, "tp", split_axis=1, concat_axis=0, tiled=True)
    ff_pair = lax.all_to_all(
        interleave(ff_gate, ff_up, n_fs), "fs", split_axis=1, concat_axis=0, tiled=True
    )
    own_down = lax.all_to_all(ff_down, "fs", split_axis=0, concat_axis=1, tiled=True)

    chans = glu_pair.shape[1] // 2
    product = jnp.dot(all_tokens, glu_pair, preferred_element_type=jnp.float32)
    glu = (product[:, :chans] * jax.nn.sigmoid(product[:, chans:])).astype(jnp.bfloat16)
    n_taps = conv_taps.shape[0]
    margin = (n_taps - 1) // 2
    own_taps = lax.dynamic_slice_in_dim(conv_taps, fs_index * chans, chans, 1)
    padded = jnp.pad(
        glu.astype(jnp.float32).reshape(groups, length, chans),
        ((0, 0), (margin, margin), (0, 0)),
    )
    conv = sum(padded[:, k : k + length] * own_taps[k] for k in range(n_taps))
    conv = conv.reshape(rows, chans).astype(jnp.bfloat16)
    conv_all = lax.all_gather(conv, ("tp", "fs"), axis=1, tiled=True)
    activated = jax.nn.silu(normed(conv_all.astype(jnp.float32)) * conv_gain_all).astype(
        jnp.bfloat16
    )
    mixed_own = jnp.dot(activated, own_out, preferred_element_type=jnp.float32).astype(
        jnp.bfloat16
    )
    mixed = lax.all_gather(mixed_own, ("fs", "tp"), axis=1, tiled=True)
    before = residual_scale * all_tokens.astype(jnp.float32) + mixed.astype(jnp.float32)
    middle = (normed(before) * mix_gain).astype(jnp.bfloat16)

    units = ff_pair.shape[1] // 2
    both = jnp.dot(middle, ff_pair, preferred_element_type=jnp.float32)
    hidden = (jax.nn.silu(both[:, :units]) * both[:, units:]).astype(jnp.bfloat16)
    down = jnp.dot(hidden, own_down, preferred_element_type=jnp.float32).astype(jnp.bfloat16)
    sends = (
        down.reshape(n_fs, seqs * length, n_tp, feat)
        .transpose(0, 2, 1, 3)
        .reshape(n_fs * n_tp, seqs * length, feat)
    )
    arrived = lax.all_to_all(sends, ("fs", "tp"), split_axis=0, concat_axis=0, tiled=True)
    forward = jnp.sum(arrived.astype(jnp.float32), axis=0)
    forward = forward.astype(jnp.bfloat16).astype(jnp.float32)
    middle_own = lax.dynamic_slice(
        middle,
        (fs_index * seqs * length, tp_index * feat),
        (seqs * length, feat),
    )
    final = residual_scale * middle_own.astype(jnp.float32) + forward
    sums, squares = lax.psum(
        (jnp.sum(final, axis=1, keepdims=True), jnp.sum(final * final, axis=1, keepdims=True)),
        "tp",
    )
    average = sums / model
    out = (final - average) * lax.rsqrt(squares / model - average * average + epsilon)
    gain = lax.dynamic_slice_in_dim(out_gain, tp_index * feat, feat, 0)
    return (out * gain).astype(jnp.bfloat16).reshape(seqs, length, feat)


MESH = pl.DeviceIdType.MESH
LANES = 128


def fused(
    n_fs,
    n_tp,
    width,
    tok,
    glu_mix,
    taps,
    gain,
    out_weight,
    mix_gain,
    gate_hbm,
    up_hbm,
    down_hbm,
    out_gain,
    out,
    x_s,
    glu_s,
    gain_s,
    proj_s,
    pad_s,
    conv_s,
    norm_s,
    act_s,
    mixed_s,
    mid_s,
    gate_s,
    up_s,
    down_s,
    hid_s,
    part_s,
    half_s,
    sum_s,
    q_s,
    stat_s,
    glu_sems,
    small_sems,
    tok_sems,
    conv_sems,
    mixed_sems,
    ff_sems,
    cross_sems,
    local_sems,
    half_sems,
    q_sems,
    y_s,
    y_sems,
    glu_cross_sems,
):
    rep, f, t = lax.axis_index("rep"), lax.axis_index("fs"), lax.axis_index("tp")
    other = 1 - t
    n_hi = n_fs // 2
    hi, lo = f // 2, f % 2
    rows, feat = x_s.shape[1:]
    length = rows // n_fs
    model = feat * n_tp
    depth = gate_hbm.shape[0]
    half_depth = depth // 2
    total = gate_hbm.shape[1]
    chans = LANES // 2
    pending = []

    barrier = pltpu.get_barrier_semaphore()
    for d in range(n_fs):
        for e in range(n_tp):
            if d or e:
                pl.semaphore_signal(
                    barrier,
                    inc=1,
                    device_id=(rep, (f + d) % n_fs, (t + e) % n_tp),
                    device_id_type=MESH,
                )
    pl.semaphore_signal(barrier, inc=1, device_id=(1 - rep, f, t), device_id_type=MESH)
    pl.semaphore_wait(barrier, n_fs * n_tp)

    def remote(src, dst, sems, index, device):
        return pltpu.make_async_remote_copy(
            src_ref=src,
            dst_ref=dst,
            send_sem=sems.at[0, index],
            recv_sem=sems.at[1, index],
            device_id=device,
            device_id_type=MESH,
        )

    def send(*parts):
        copy = remote(*parts)
        copy.start()
        pending.append(copy)

    partner = (rep, f, other)

    def receive(dst, sems, index):
        remote(dst, dst, sems, index, partner).wait_recv()

    def at(step, low):
        return ((hi - step + n_hi) % n_hi) * 2 + low

    def gather_start(own, slot, sems):
        for d in range(1, n_hi):
            send(own, slot(f, t), sems, d, (rep, ((hi + d) % n_hi) * 2 + lo, t))
        send(own, slot(f, t), sems, n_hi, (rep, hi * 2 + 1 - lo, t))
        send(own, slot(f, t), sems, 2 * n_hi, partner)

    def gather_finish(slot, sems):
        for d in range(1, n_hi):
            block = slot(at(d, lo), t)
            receive(block, sems, d)
            send(block, block, sems, n_hi + d, (rep, hi * 2 + 1 - lo, t))
            send(block, block, sems, 2 * n_hi + d, partner)
        for d in range(n_hi):
            block = slot(at(d, 1 - lo), t)
            receive(block, sems, n_hi + d)
            send(block, block, sems, 3 * n_hi + d, partner)
        for d in range(n_hi):
            receive(slot(at(d, lo), other), sems, 2 * n_hi + d)
            receive(slot(at(d, 1 - lo), other), sems, 3 * n_hi + d)

    def tok_slot(i, j):
        return x_s.at[j, pl.ds(pl.multiple_of(i * length, length), length)]

    def half_rows(i, part):
        return pl.ds(pl.multiple_of(i * depth + part * half_depth, half_depth), half_depth)

    gather_start(tok, tok_slot, tok_sems)
    for d in range(1, n_fs):
        to = (f + d) % n_fs
        send(
            glu_mix.at[to, half_rows(0, rep)],
            glu_s.at[half_rows(f, rep)],
            glu_sems,
            d,
            (rep, to, t),
        )
    send(gain, gain_s.at[t], small_sems, 0, partner)
    columns = pl.ds(pl.multiple_of(other * LANES, LANES), LANES)
    own_columns = pl.ds(pl.multiple_of(t * LANES, LANES), LANES)
    send(out_weight.at[:, columns], proj_s.at[t], small_sems, 1, partner)

    def start_of(i):
        return pl.multiple_of(i * width - (i // (n_fs - 1)) * (n_fs * width - total), LANES)

    half_width = width // 2

    def pieces(to, source, part):
        first = start_of(to)
        ups = pl.ds(pl.multiple_of(part * half_depth, half_depth), half_depth)
        spot = pl.ds(pl.multiple_of(source * depth + part * half_depth, half_depth), half_depth)
        deep = pl.ds(pl.multiple_of(part * half_width, half_width), half_width)
        from_down = pl.ds(pl.multiple_of(first + part * half_width, LANES // 2), half_width)
        return (
            (gate_hbm.at[ups, pl.ds(first, width)], gate_s.at[spot]),
            (up_hbm.at[ups, pl.ds(first, width)], up_s.at[spot]),
            (down_hbm.at[from_down], down_s.at[source, deep]),
        )

    order = range(1, n_fs)
    early, late = range(1, n_fs // 2 + 1), range(n_fs // 2 + 1, n_fs)

    def weights_start(which, order=order):
        for d in order:
            to = (f + d) % n_fs
            src, dst = pieces(to, f, rep)[which]
            send(src, dst, ff_sems, which * n_fs + d, (rep, to, t))

    def weights_forward(which, order=order):
        for d in order:
            dst = pieces(f, (f - d + n_fs) % n_fs, rep)[which][1]
            receive(dst, ff_sems, which * n_fs + d)
            send(dst, dst, cross_sems, which * n_fs + d, (1 - rep, f, t))

    def weights_finish(which):
        for d in order:
            dst = pieces(f, (f - d + n_fs) % n_fs, 1 - rep)[which][1]
            receive(dst, cross_sems, which * n_fs + d)

    weights_start(0)
    weights_start(1)
    own_copies = []
    for which in range(3):
        for part in range(2):
            src, dst = pieces(f, f, part)[which]
            own_copies.append(
                pltpu.make_async_copy(src, dst, local_sems.at[which * 2 + part])
            )
    for copy in own_copies:
        copy.start()

    x_s[t, pl.ds(pl.multiple_of(f * length, length), length), :] = tok[...]
    glu_s[pl.ds(pl.multiple_of(f * depth, depth), depth), :] = glu_mix[f]
    gain_s[t] = gain[...]
    proj_s[t] = out_weight[:, own_columns]
    pad_s[...] = jnp.zeros_like(pad_s)

    gather_finish(tok_slot, tok_sems)
    for d in range(1, n_fs):
        block = glu_s.at[half_rows((f - d + n_fs) % n_fs, rep)]
        receive(block, glu_sems, d)
        send(block, block, glu_cross_sems, d, (1 - rep, f, t))
    for d in range(1, n_fs):
        block = glu_s.at[half_rows((f - d + n_fs) % n_fs, 1 - rep)]
        receive(block, glu_cross_sems, d)

    product = sum(
        jnp.dot(
            x_s[j], glu_s[j * feat : (j + 1) * feat], preferred_element_type=jnp.float32
        )
        for j in range(n_tp)
    )
    glu = product[:, :chans] / (1.0 + jnp.exp(-product[:, chans:]))
    top = rows // 2
    packed = jnp.concatenate((glu[:top], glu[top:]), axis=1)
    packed = packed.astype(jnp.bfloat16).astype(jnp.float32)
    n_taps = taps.shape[0]
    margin = (n_taps - 1) // 2
    conv_slot = lambda i, j: conv_s.at[j * n_fs + i]
    groups = n_fs // 2
    for g in range(groups):
        pad_s[g, 16 : 16 + length, :] = packed[g * length : (g + 1) * length]
    for g in range(groups):
        acc = jnp.zeros((length, LANES), jnp.float32)
        for k in range(n_taps):
            first = 16 - margin + k
            acc = acc + pad_s[g, first : first + length, :] * taps[k : k + 1, :]
        conv_s[t * n_fs + f, g * length : (g + 1) * length, :] = acc.astype(jnp.bfloat16)
    gather_start(conv_slot(f, t), conv_slot, conv_sems)
    weights_start(2, early)
    weights_forward(0)
    weights_forward(1)
    gather_finish(conv_slot, conv_sems)
    receive(gain_s.at[other], small_sems, 0)
    receive(proj_s.at[other], small_sems, 1)

    for j in range(n_fs * n_tp // 2):
        left = conv_s[2 * j].astype(jnp.float32)
        right = conv_s[2 * j + 1].astype(jnp.float32)
        cols = slice(j * LANES, (j + 1) * LANES)
        norm_s[:top, cols] = jnp.concatenate((left[:, :chans], right[:, :chans]), axis=1)
        norm_s[top:, cols] = jnp.concatenate((left[:, chans:], right[:, chans:]), axis=1)
    gains = jnp.concatenate([gain_s[j] for j in range(n_tp)], axis=1)

    @pl.loop(0, n_fs)
    def _(i):
        here = pl.ds(pl.multiple_of(i * length, length), length)
        v = normed(norm_s[here, :]) * gains
        act_s[here, :] = (v / (1.0 + jnp.exp(-v))).astype(jnp.bfloat16)

    share = proj_s.shape[1]
    mixed_slot = lambda i, j: mixed_s.at[i * n_tp + j]
    mixed_s[f * n_tp + t] = sum(
        jnp.dot(
            act_s[:, j * share : (j + 1) * share],
            proj_s[j],
            preferred_element_type=jnp.float32,
        )
        for j in range(n_tp)
    ).astype(jnp.bfloat16)
    gather_start(mixed_slot(f, t), mixed_slot, mixed_sems)
    weights_start(2, late)
    weights_forward(2, early)
    gather_finish(mixed_slot, mixed_sems)

    @pl.loop(0, n_fs)
    def _(i):
        here = pl.ds(pl.multiple_of(i * length, length), length)
        skip = jnp.concatenate([x_s[j, here, :] for j in range(n_tp)], axis=1)
        added = jnp.concatenate([mixed_s[j, here, :] for j in range(n_fs * n_tp)], axis=1)
        before = residual_scale * skip.astype(jnp.float32) + added.astype(jnp.float32)
        mid_s[here, :] = (normed(before) * mix_gain[...]).astype(jnp.bfloat16)

    for copy in own_copies:
        copy.wait()
    weights_finish(0)
    weights_finish(1)
    keep = lax.broadcasted_iota(jnp.int32, (1, width), 1) + start_of(f) >= f * width

    for i in range(2):
        here = pl.ds(i * top, top)
        gate = jnp.dot(mid_s[here, :], gate_s[...], preferred_element_type=jnp.float32)
        upward = jnp.dot(mid_s[here, :], up_s[...], preferred_element_type=jnp.float32)
        value = gate / (1.0 + jnp.exp(-gate)) * upward
        hid_s[here, :] = jnp.where(keep, value, 0.0).astype(jnp.bfloat16)
        if i == 0:
            weights_forward(2, late)

    weights_finish(2)
    span = down_s.shape[2]
    per_half = n_fs // n_tp

    def project(side):
        @pl.loop(0, per_half)
        def _(j):
            part_s[side, :, pl.ds(pl.multiple_of(j * span, span), span)] = jnp.dot(
                hid_s[...], down_s[side * per_half + j], preferred_element_type=jnp.float32
            ).astype(jnp.bfloat16)

    def rows_of(i):
        return pl.ds(pl.multiple_of(i * length, length), length)

    def toward(step, low):
        return ((hi + step) % n_hi) * 2 + low

    steps = list(range(1, n_hi)) + [0]
    project(other)
    for d in steps:
        for e, low in enumerate((1 - lo, lo)):
            here = rows_of(toward(d, low))
            send(part_s.at[other, here], half_s.at[here], half_sems, 2 * d + e, partner)
    project(t)
    for d in steps:
        here = rows_of(toward(d, 1 - lo))
        receive(half_s.at[here], half_sems, 2 * d)
        both = part_s[t, here, :].astype(jnp.float32) + half_s[here, :].astype(jnp.float32)
        sum_s[here, :] = both.astype(jnp.bfloat16)
        send(sum_s.at[here], y_s.at[d], y_sems, d, (rep, hi * 2 + 1 - lo, t))
    for d in steps:
        to = toward(d, lo)
        here = rows_of(to)
        receive(half_s.at[here], half_sems, 2 * d + 1)
        both = part_s[t, here, :].astype(jnp.float32) + half_s[here, :].astype(jnp.float32)
        receive(y_s.at[d], y_sems, d)
        forward = both + y_s[d].astype(jnp.float32)
        if d:
            sum_s[here, :] = forward.astype(jnp.bfloat16)
            send(sum_s.at[here], q_s.at[d], q_sems, d, (rep, to, t))
    for d in range(1, n_hi):
        receive(q_s.at[d], q_sems, d)
        forward = forward + q_s[d].astype(jnp.float32)
    forward = forward.astype(jnp.bfloat16).astype(jnp.float32)
    own_half = pl.ds(pl.multiple_of(t * feat, feat), feat)
    final = residual_scale * mid_s[rows_of(f), own_half].astype(jnp.float32) + forward
    lane = lax.broadcasted_iota(jnp.int32, (length, LANES), 1)
    stat_s[t] = jnp.where(
        lane == 0,
        jnp.sum(final, axis=1, keepdims=True),
        jnp.sum(final * final, axis=1, keepdims=True),
    )
    send(stat_s.at[t], stat_s.at[t], small_sems, 2, partner)
    receive(stat_s.at[other], small_sems, 2)
    stats = (stat_s[0] + stat_s[1]) / model
    average, second = stats[:, 0:1], stats[:, 1:2]
    scaled = (final - average) * lax.rsqrt(second - average * average + epsilon)
    out[...] = (scaled * out_gain[t]).astype(jnp.bfloat16)
    for copy in pending:
        copy.wait_send()


def by_kernel(
    width,
    tokens,
    lin_weight,
    glu_weight,
    conv_taps,
    conv_gain,
    conv_out_weight,
    mix_gain,
    ff_gate,
    ff_up,
    ff_down,
    out_gain,
):
    n_fs, n_tp = lax.axis_size("fs"), lax.axis_size("tp")
    _, length, feat = tokens.shape
    rows, model = n_fs * length, feat * n_tp
    depth, own_chans = lin_weight.shape
    chans = own_chans // n_fs
    n_taps = conv_taps.shape[0]
    glu_mix = jnp.concatenate(
        (
            lin_weight.reshape(depth, n_fs, chans).transpose(1, 0, 2),
            glu_weight.reshape(depth, n_fs, chans).transpose(1, 0, 2),
        ),
        axis=2,
    )
    own_taps = lax.dynamic_slice_in_dim(conv_taps, lax.axis_index("fs") * chans, chans, 1)
    taps = jnp.concatenate((own_taps, own_taps), axis=1)
    vmem, far = pl.BlockSpec(memory_space=pltpu.VMEM), pl.BlockSpec(memory_space=pl.ANY)
    bf, fl = jnp.bfloat16, jnp.float32
    span = ff_down.shape[1]
    pair = lambda n: pltpu.SemaphoreType.DMA((2, n))
    result = pl.pallas_call(
        functools.partial(fused, n_fs, n_tp, width),
        out_shape=jax.ShapeDtypeStruct((length, feat), bf),
        in_specs=[vmem] * 6 + [far] * 3 + [vmem],
        out_specs=vmem,
        scratch_shapes=[
            pltpu.VMEM((n_tp, rows, feat), bf),
            pltpu.VMEM((n_fs * depth, 2 * chans), bf),
            pltpu.VMEM((n_tp, 1, own_chans), fl),
            pltpu.VMEM((n_tp, own_chans, span // n_tp), bf),
            pltpu.VMEM((n_fs // 2, length + 32, LANES), fl),
            pltpu.VMEM((n_fs * n_tp, rows // 2, LANES), bf),
            pltpu.VMEM((rows, own_chans * n_tp), fl),
            pltpu.VMEM((rows, own_chans * n_tp), bf),
            pltpu.VMEM((n_fs * n_tp, rows, LANES), bf),
            pltpu.VMEM((rows, model), bf),
            pltpu.VMEM((n_fs * depth, width), bf),
            pltpu.VMEM((n_fs * depth, width), bf),
            pltpu.VMEM((n_fs, width, span), bf),
            pltpu.VMEM((rows, width), bf),
            pltpu.VMEM((n_tp, rows, feat), bf),
            pltpu.VMEM((rows, feat), bf),
            pltpu.VMEM((rows, feat), bf),
            pltpu.VMEM((n_fs // 2, length, feat), bf),
            pltpu.VMEM((n_tp, length, LANES), fl),
            pair(n_fs),
            pair(3),
            pair(2 * n_fs),
            pair(2 * n_fs),
            pair(2 * n_fs),
            pair(3 * n_fs),
            pair(3 * n_fs),
            pltpu.SemaphoreType.DMA((6,)),
            pair(n_fs),
            pair(n_fs // 2),
            pltpu.VMEM((n_fs // 2, length, feat), bf),
            pair(n_fs // 2),
            pair(n_fs),
        ],
        compiler_params=pltpu.CompilerParams(
            collective_id=0, has_side_effects=True, vmem_limit_bytes=60 * 2**20
        ),
    )(
        tokens[0],
        glu_mix,
        taps,
        conv_gain[None],
        conv_out_weight,
        mix_gain[None],
        ff_gate,
        ff_up,
        ff_down,
        out_gain.reshape(n_tp, 1, feat),
    )
    return result[None]


def on_device(*args):
    tokens, lin_weight, conv_out_weight, ff_gate = args[0], args[1], args[5], args[7]
    n_fs, n_tp, n_rep = (lax.axis_size(a) for a in ("fs", "tp", "rep"))
    seqs, length, feat = tokens.shape
    units = ff_gate.shape[1]
    width = -(-units // (n_fs * LANES)) * LANES
    fits = (
        n_rep == 2
        and n_tp == 2
        and n_fs % 4 == 0
        and seqs == 1
        and length % 16 == 0
        and args[3].shape[0] <= 33
        and lin_weight.shape[1] * 2 == n_fs * LANES
        and conv_out_weight.shape[1] == n_tp * LANES
        and feat % LANES == 0
        and units % LANES == 0
        and width * (n_fs - 1) < units
        and lin_weight.shape[0] % 32 == 0
    )
    if fits:
        return by_kernel(width, *args)
    return by_collectives(*args)


def solution(mesh):
    mapped = jax.shard_map(
        on_device,
        mesh=mesh,
        in_specs=(
            P(("rep", "fs"), None, "tp"),
            P("fs", "tp"),
            P("fs", "tp"),
            P(None, "tp"),
            P("tp"),
            P("tp", "fs"),
            P(),
            P("fs", "tp"),
            P("fs", "tp"),
            P("tp", "fs"),
            P(),
        ),
        out_specs=P(("rep", "fs"), None, "tp"),
        check_vma=False,
    )
    return mapped
```

profile of v0, /device:TPU:11, one launch (start us, length us, event | category | flops | bytes accessed | tf_op | source)
XLA Modules:
  0.0 144.7 jit_solution(14268505137644296270)
XLA Ops:
  0.0 0.0 copy-start
  0.0 0.0 copy-start.1
  0.0 1.1 copy.14
  1.1 0.3 copy.15
  1.4 0.0 copy-done.1
  1.4 0.1 copy.12
  1.6 0.3 copy.13
  1.9 1.1 pad_maximum_fusion.glu_mix
  2.9 0.0 copy-done
  2.9 0.1 constant_dynamic-slice_fusion
  3.0 0.7 pad_maximum_fusion.1.taps
  3.7 139.4 %shard_map.109 = bf16[64,1024]{1,0:T(8,128)(2,1)} custom-call(bf16[64,1024]{1,0:T(8,128)(2,1)} %bitcast.14, bf16[8,256,128]{2,1,0:T(8,128)(2,1)} %pad_maximum_fusion.glu_mix, f32[31,128]{1,0:T(8,128)} %pad_maximum_fusion.1.taps, f32[1,512]{1,0:T(1,128)} %bitcast.17, bf16[512,256]{1,0:T(8,128)(2,1)} %out_weight.1, f32[1,2048]{1,0:T(1,128)} %bitcast.15, ...), custom_call_target="tpu_custom_call" | custom-call | tf_op jit(solution)/shard_map/pallas_call | solution.py:499
  143.1 1.6 %copy.17 = bf16[1,64,1024]{2,1,0:T(8,128)(2,1)} copy(bf16[1,64,1024]{2,1,0:T(8,128)(2,1)} %bitcast.13) | data formatting | bytes 262144
Async XLA Ops:
  0.0 2.9 %copy-start = (f32[31,512]{1,0:T(8,128)S(1)}, f32[31,512]{1,0:T(8,128)}, u32[]{:S(2)}) copy-start(f32[31,512]{1,0:T(8,128)} %param.14) | copy-start | bytes 190468
  0.0 1.4 copy-start.1
where the time goes:
time: 145 us
  Pallas kernels  139 us (96%)
  local copies, waits for them, and re-layouts  3.46 us (2%)
  other arithmetic  1.76 us (1%)
    pallas_call x1, Pallas kernels, by_kernel(): pl.pallas_call(functools.partial(fused, n_fs, n_tp, width), out_shape=jax...  139 us

commit v1 on v0

--- a/solution.py
+++ b/solution.py
@@ -115,15 +115,46 @@
 
 MESH = pl.DeviceIdType.MESH
 LANES = 128
-
+FIRST = ((2, 0), (3, 0))
+CROSS = ((2, 1), (3, 1))
+NEAR = ((1, 0), (1, 1), (0, 1))
+OTHERS = FIRST + CROSS + NEAR
+G, U, D = 0, 1, 2
+SENDS = {
+    "t0": ((G, 2, 0),),
+    "t3": ((U, 2, 0),),
+    "t5": ((G, 3, 0), (G, 1, 0), (U, 3, 0)),
+    "t7": ((G, 0, 1),),
+    "c0": ((G, 2, 1),),
+    "c5": ((U, 2, 1), (U, 1, 0)),
+    "c7": ((G, 3, 1), (U, 0, 1), (G, 1, 1)),
+    "m0": ((U, 3, 1),),
+    "m3": ((U, 1, 1), (D, 2, 0)),
+    "m5": ((D, 3, 0),),
+    "m7": ((D, 2, 1), (D, 3, 1), (D, 1, 0), (D, 1, 1), (D, 0, 1)),
+}
+FORWARDS = {
+    "c0": ((G, 2, 0), (U, 2, 0)),
+    "c4": ((G, 3, 0),),
+    "c6": ((G, 1, 0), (U, 3, 0), (G, 0, 1)),
+    "m0": ((G, 2, 1),),
+    "m2": ((U, 2, 1), (U, 1, 0)),
+    "m4": ((G, 3, 1), (U, 0, 1)),
+    "m6": ((G, 1, 1), (U, 3, 1)),
+    "m8": ((U, 1, 1), (D, 2, 0)),
+    "f0": ((D, 3, 0),),
+    "f1": ((D, 2, 1), (D, 3, 1), (D, 1, 0), (D, 1, 1), (D, 0, 1)),
+}
 
 def fused(
     n_fs,
     n_tp,
     width,
+    narrow,
     tok,
-    glu_mix,
-    taps,
+    lin_hbm,
+    glu_hbm,
+    taps_hbm,
     gain,
     out_weight,
     mix_gain,
@@ -133,6 +164,10 @@
     out_gain,
     out,
     x_s,
+    lin_s,
+    gl_s,
+    taps_s,
+    mix_s,
     glu_s,
     gain_s,
     proj_s,
@@ -150,8 +185,10 @@
     half_s,
     sum_s,
     q_s,
+    y_s,
     stat_s,
     glu_sems,
+    glu_cross_sems,
     small_sems,
     tok_sems,
     conv_sems,
@@ -161,9 +198,7 @@
     local_sems,
     half_sems,
     q_sems,
-    y_s,
     y_sems,
-    glu_cross_sems,
 ):
     rep, f, t = lax.axis_index("rep"), lax.axis_index("fs"), lax.axis_index("tp")
     other = 1 - t
@@ -174,22 +209,85 @@
     model = feat * n_tp
     depth = gate_hbm.shape[0]
     half_depth = depth // 2
-    total = gate_hbm.shape[1]
     chans = LANES // 2
     pending = []
 
+    def flip(z, step):
+        return z + step - 2 * step * ((z // step) % 2)
+
+    def along(k):
+        z = hi
+        for step in (1, 2):
+            if k[0] & step:
+                z = flip(z, step)
+        return z * 2 + (1 - lo if k[1] else lo)
+
+    def code(k):
+        return k[0] * 2 + k[1]
+
     barrier = pltpu.get_barrier_semaphore()
-    for d in range(n_fs):
-        for e in range(n_tp):
-            if d or e:
-                pl.semaphore_signal(
-                    barrier,
-                    inc=1,
-                    device_id=(rep, (f + d) % n_fs, (t + e) % n_tp),
-                    device_id_type=MESH,
-                )
+    for k in OTHERS:
+        pl.semaphore_signal(barrier, inc=1, device_id=(rep, along(k), t), device_id_type=MESH)
+    pl.semaphore_signal(barrier, inc=1, device_id=(rep, f, other), device_id_type=MESH)
     pl.semaphore_signal(barrier, inc=1, device_id=(1 - rep, f, t), device_id_type=MESH)
-    pl.semaphore_wait(barrier, n_fs * n_tp)
+
+    def rows_of(i):
+        return pl.ds(pl.multiple_of(i * length, length), length)
+
+    def depth_of(i, part, size):
+        return pl.ds(pl.multiple_of(i * depth + part * half_depth, half_depth), size)
+
+    def tok_slot(i, j):
+        return x_s.at[j, rows_of(i)]
+
+    per_half = n_fs // 2
+
+    def start_of(i):
+        return pl.multiple_of((i * (width // LANES) - i // per_half) * LANES, LANES)
+
+    def is_short(i):
+        return i % per_half == per_half - 1
+
+    def sized(i, action):
+        @pl.when(jnp.logical_not(is_short(i)))
+        def _():
+            action(width)
+
+        @pl.when(is_short(i))
+        def _():
+            action(narrow)
+
+    fetches = [
+        pltpu.make_async_copy(src, dst, local_sems.at[n])
+        for n, (src, dst) in enumerate(
+            (
+                (tok, tok_slot(f, t)),
+                (lin_hbm, lin_s),
+                (glu_hbm, gl_s),
+                (taps_hbm, taps_s),
+            )
+        )
+    ]
+    for copy in fetches:
+        copy.start()
+
+    def own_copy(which, size):
+        first = start_of(f)
+        src, dst = (
+            (gate_hbm.at[:, pl.ds(first, size)], gate_s.at[depth_of(f, 0, depth), pl.ds(0, size)]),
+            (up_hbm.at[:, pl.ds(first, size)], up_s.at[depth_of(f, 0, depth), pl.ds(0, size)]),
+            (down_hbm.at[pl.ds(first, size)], down_s.at[f, pl.ds(0, size)]),
+        )[which]
+        return pltpu.make_async_copy(src, dst, local_sems.at[4 + which])
+
+    for which in range(3):
+        sized(f, lambda size, which=which: own_copy(which, size).start())
+
+    @pl.when(is_short(f))
+    def _():
+        gate_s[:, narrow:] = jnp.zeros((n_fs * depth, width - narrow), jnp.bfloat16)
+        up_s[:, narrow:] = jnp.zeros((n_fs * depth, width - narrow), jnp.bfloat16)
+        down_s[:, narrow:, :] = jnp.zeros((n_fs, width - narrow, down_s.shape[2]), jnp.bfloat16)
 
     def remote(src, dst, sems, index, device):
         return pltpu.make_async_remote_copy(
@@ -204,120 +302,169 @@
     def send(*parts):
         copy = remote(*parts)
         copy.start()
-        pending.append(copy)
+        pending.append(copy.wait_send)
 
     partner = (rep, f, other)
+    mirror = (1 - rep, f, t)
+    beside = (rep, along((0, 1)), t)
+    close = (rep, along((1, 0)), t)
+    far = (rep, along((2, 0)), t)
 
     def receive(dst, sems, index):
         remote(dst, dst, sems, index, partner).wait_recv()
 
-    def at(step, low):
-        return ((hi - step + n_hi) % n_hi) * 2 + low
-
-    def gather_start(own, slot, sems):
-        for d in range(1, n_hi):
-            send(own, slot(f, t), sems, d, (rep, ((hi + d) % n_hi) * 2 + lo, t))
-        send(own, slot(f, t), sems, n_hi, (rep, hi * 2 + 1 - lo, t))
-        send(own, slot(f, t), sems, 2 * n_hi, partner)
-
-    def gather_finish(slot, sems):
-        for d in range(1, n_hi):
-            block = slot(at(d, lo), t)
-            receive(block, sems, d)
-            send(block, block, sems, n_hi + d, (rep, hi * 2 + 1 - lo, t))
-            send(block, block, sems, 2 * n_hi + d, partner)
-        for d in range(n_hi):
-            block = slot(at(d, 1 - lo), t)
-            receive(block, sems, n_hi + d)
-            send(block, block, sems, 3 * n_hi + d, partner)
-        for d in range(n_hi):
-            receive(slot(at(d, lo), other), sems, 2 * n_hi + d)
-            receive(slot(at(d, 1 - lo), other), sems, 3 * n_hi + d)
-
-    def tok_slot(i, j):
-        return x_s.at[j, pl.ds(pl.multiple_of(i * length, length), length)]
-
-    def half_rows(i, part):
-        return pl.ds(pl.multiple_of(i * depth + part * half_depth, half_depth), half_depth)
-
-    gather_start(tok, tok_slot, tok_sems)
-    for d in range(1, n_fs):
-        to = (f + d) % n_fs
-        send(
-            glu_mix.at[to, half_rows(0, rep)],
-            glu_s.at[half_rows(f, rep)],
-            glu_sems,
-            d,
-            (rep, to, t),
+    def gather_start(slot, sems):
+        block = slot(f, t)
+        send(block, block, sems, 0, far)
+        send(block, block, sems, 1, close)
+        send(block, block, sems, 3, beside)
+        send(block, block, sems, 7, partner)
+
+    def slot(name):
+        for which, *k in SENDS.get(name, ()):
+            weight_send(which, tuple(k))
+        for which, *k in FORWARDS.get(name, ()):
+            weight_forward(which, tuple(k))
+
+    def gather_finish(place, sems, name, between=None):
+        between = between or {}
+
+        def pause(step):
+            slot(name + str(step))
+            if step in between:
+                between[step]()
+
+        def got(index, k):
+            block = place(along(k), t)
+            receive(block, sems, index)
+            return block
+
+        block = got(1, (1, 0))
+        send(block, block, sems, 4, beside)
+        send(block, block, sems, 7 + code((1, 0)), partner)
+        pause(1)
+        block = got(3, (0, 1))
+        send(block, block, sems, 7 + code((0, 1)), partner)
+        pause(2)
+        block = got(0, (2, 0))
+        send(block, block, sems, 2, close)
+        send(block, block, sems, 5, beside)
+        send(block, block, sems, 7 + code((2, 0)), partner)
+        pause(3)
+        block = got(4, (1, 1))
+        send(block, block, sems, 7 + code((1, 1)), partner)
+        pause(4)
+        block = got(2, (3, 0))
+        send(block, block, sems, 6, beside)
+        send(block, block, sems, 7 + code((3, 0)), partner)
+        pause(5)
+        block = got(5, (2, 1))
+        send(block, block, sems, 7 + code((2, 1)), partner)
+        pause(6)
+        block = got(6, (3, 1))
+        send(block, block, sems, 7 + code((3, 1)), partner)
+        pause(7)
+        for k in ((0, 0),) + OTHERS:
+            receive(place(along(k), other), sems, 7 + code(k))
+
+    half_width = width // 2
+
+    def piece(which, to, source, part, size):
+        first = start_of(to)
+        ups = pl.ds(pl.multiple_of(part * half_depth, half_depth), half_depth)
+        spot = depth_of(source, part, half_depth)
+        deep = pl.ds(pl.multiple_of(part * (size // 2), size // 2), size // 2)
+        from_down = pl.ds(pl.multiple_of(first + part * (size // 2), LANES // 2), size // 2)
+        return (
+            (gate_hbm.at[ups, pl.ds(first, size)], gate_s.at[spot, pl.ds(0, size)]),
+            (up_hbm.at[ups, pl.ds(first, size)], up_s.at[spot, pl.ds(0, size)]),
+            (down_hbm.at[from_down], down_s.at[source, deep]),
+        )[which]
+
+    def weight_send(which, k):
+        to = along(k)
+
+        def copy(size):
+            src, dst = piece(which, to, f, rep, size)
+            return remote(src, dst, ff_sems, which * n_fs + code(k), (rep, to, t))
+
+        sized(to, lambda size: copy(size).start())
+        pending.append(lambda: sized(to, lambda size: copy(size).wait_send()))
+
+    def weight_forward(which, k):
+        index = which * n_fs + code(k)
+
+        def block(size):
+            return piece(which, f, along(k), rep, size)[1]
+
+        def action(size):
+            receive(block(size), ff_sems, index)
+            remote(block(size), block(size), cross_sems, index, mirror).start()
+
+        sized(f, action)
+        pending.append(
+            lambda: sized(
+                f,
+                lambda size: remote(
+                    block(size), block(size), cross_sems, index, mirror
+                ).wait_send(),
+            )
         )
-    send(gain, gain_s.at[t], small_sems, 0, partner)
+
+    def weight_finish(which):
+        for k in OTHERS:
+            sized(
+                f,
+                lambda size: receive(
+                    piece(which, f, along(k), 1 - rep, size)[1], cross_sems, which * n_fs + code(k)
+                ),
+            )
+
+    pl.semaphore_wait(barrier, n_fs + 1)
+    fetches[0].wait()
+    gather_start(tok_slot, tok_sems)
+    fetches[1].wait()
+    fetches[2].wait()
+    for d in range(n_fs):
+        cols = slice(d * chans, (d + 1) * chans)
+        mix_s[d] = jnp.concatenate((lin_s[:, cols], gl_s[:, cols]), axis=1)
+
+    def glu_piece(source, part):
+        return glu_s.at[depth_of(source, part, half_depth)]
+
+    for k in OTHERS:
+        to = along(k)
+        own_rows = pl.ds(pl.multiple_of(rep * half_depth, half_depth), half_depth)
+        send(mix_s.at[to, own_rows], glu_piece(f, rep), glu_sems, code(k), (rep, to, t))
+    slot("t0")
     columns = pl.ds(pl.multiple_of(other * LANES, LANES), LANES)
     own_columns = pl.ds(pl.multiple_of(t * LANES, LANES), LANES)
+    send(gain, gain_s.at[t], small_sems, 0, partner)
     send(out_weight.at[:, columns], proj_s.at[t], small_sems, 1, partner)
 
-    def start_of(i):
-        return pl.multiple_of(i * width - (i // (n_fs - 1)) * (n_fs * width - total), LANES)
-
-    half_width = width // 2
-
-    def pieces(to, source, part):
-        first = start_of(to)
-        ups = pl.ds(pl.multiple_of(part * half_depth, half_depth), half_depth)
-        spot = pl.ds(pl.multiple_of(source * depth + part * half_depth, half_depth), half_depth)
-        deep = pl.ds(pl.multiple_of(part * half_width, half_width), half_width)
-        from_down = pl.ds(pl.multiple_of(first + part * half_width, LANES // 2), half_width)
-        return (
-            (gate_hbm.at[ups, pl.ds(first, width)], gate_s.at[spot]),
-            (up_hbm.at[ups, pl.ds(first, width)], up_s.at[spot]),
-            (down_hbm.at[from_down], down_s.at[source, deep]),
-        )
-
-    order = range(1, n_fs)
-    early, late = range(1, n_fs // 2 + 1), range(n_fs // 2 + 1, n_fs)
-
-    def weights_start(which, order=order):
-        for d in order:
-            to = (f + d) % n_fs
-            src, dst = pieces(to, f, rep)[which]
-            send(src, dst, ff_sems, which * n_fs + d, (rep, to, t))
-
-    def weights_forward(which, order=order):
-        for d in order:
-            dst = pieces(f, (f - d + n_fs) % n_fs, rep)[which][1]
-            receive(dst, ff_sems, which * n_fs + d)
-            send(dst, dst, cross_sems, which * n_fs + d, (1 - rep, f, t))
-
-    def weights_finish(which):
-        for d in order:
-            dst = pieces(f, (f - d + n_fs) % n_fs, 1 - rep)[which][1]
-            receive(dst, cross_sems, which * n_fs + d)
-
-    weights_start(0)
-    weights_start(1)
-    own_copies = []
-    for which in range(3):
-        for part in range(2):
-            src, dst = pieces(f, f, part)[which]
-            own_copies.append(
-                pltpu.make_async_copy(src, dst, local_sems.at[which * 2 + part])
-            )
-    for copy in own_copies:
-        copy.start()
-
-    x_s[t, pl.ds(pl.multiple_of(f * length, length), length), :] = tok[...]
-    glu_s[pl.ds(pl.multiple_of(f * depth, depth), depth), :] = glu_mix[f]
+    glu_s[pl.ds(pl.multiple_of(f * depth, depth), depth), :] = mix_s[f]
     gain_s[t] = gain[...]
     proj_s[t] = out_weight[:, own_columns]
     pad_s[...] = jnp.zeros_like(pad_s)
 
-    gather_finish(tok_slot, tok_sems)
-    for d in range(1, n_fs):
-        block = glu_s.at[half_rows((f - d + n_fs) % n_fs, rep)]
-        receive(block, glu_sems, d)
-        send(block, block, glu_cross_sems, d, (1 - rep, f, t))
-    for d in range(1, n_fs):
-        block = glu_s.at[half_rows((f - d + n_fs) % n_fs, 1 - rep)]
-        receive(block, glu_cross_sems, d)
+    def glu_forward(ks):
+        for k in ks:
+            block = glu_piece(along(k), rep)
+            receive(block, glu_sems, code(k))
+            send(block, block, glu_cross_sems, code(k), mirror)
+
+    gather_finish(
+        tok_slot,
+        tok_sems,
+        "t",
+        {
+            4: lambda: glu_forward(NEAR),
+            5: lambda: glu_forward(FIRST),
+            6: lambda: glu_forward(CROSS),
+        },
+    )
+    for k in OTHERS:
+        receive(glu_piece(along(k), 1 - rep), glu_cross_sems, code(k))
 
     product = sum(
         jnp.dot(
@@ -329,6 +476,11 @@
     top = rows // 2
     packed = jnp.concatenate((glu[:top], glu[top:]), axis=1)
     packed = packed.astype(jnp.bfloat16).astype(jnp.float32)
+    fetches[3].wait()
+    lanes = lax.broadcasted_iota(jnp.int32, (1, LANES), 1)
+    tap_pair = taps_s[:, pl.ds(pl.multiple_of(f // 2 * LANES, LANES), LANES)]
+    turned = pltpu.roll(tap_pair, chans, 1)
+    taps = jnp.where((lanes < chans) == (f % 2 == 0), tap_pair, turned)
     n_taps = taps.shape[0]
     margin = (n_taps - 1) // 2
     conv_slot = lambda i, j: conv_s.at[j * n_fs + i]
@@ -341,11 +493,9 @@
             first = 16 - margin + k
             acc = acc + pad_s[g, first : first + length, :] * taps[k : k + 1, :]
         conv_s[t * n_fs + f, g * length : (g + 1) * length, :] = acc.astype(jnp.bfloat16)
-    gather_start(conv_slot(f, t), conv_slot, conv_sems)
-    weights_start(2, early)
-    weights_forward(0)
-    weights_forward(1)
-    gather_finish(conv_slot, conv_sems)
+    gather_start(conv_slot, conv_sems)
+    slot("c0")
+    gather_finish(conv_slot, conv_sems, "c")
     receive(gain_s.at[other], small_sems, 0)
     receive(proj_s.at[other], small_sems, 1)
 
@@ -359,7 +509,7 @@
 
     @pl.loop(0, n_fs)
     def _(i):
-        here = pl.ds(pl.multiple_of(i * length, length), length)
+        here = rows_of(i)
         v = normed(norm_s[here, :]) * gains
         act_s[here, :] = (v / (1.0 + jnp.exp(-v))).astype(jnp.bfloat16)
 
@@ -373,47 +523,44 @@
         )
         for j in range(n_tp)
     ).astype(jnp.bfloat16)
-    gather_start(mixed_slot(f, t), mixed_slot, mixed_sems)
-    weights_start(2, late)
-    weights_forward(2, early)
-    gather_finish(mixed_slot, mixed_sems)
+    gather_start(mixed_slot, mixed_sems)
+    slot("m0")
+    gather_finish(mixed_slot, mixed_sems, "m")
+    slot("m8")
 
     @pl.loop(0, n_fs)
     def _(i):
-        here = pl.ds(pl.multiple_of(i * length, length), length)
+        here = rows_of(i)
         skip = jnp.concatenate([x_s[j, here, :] for j in range(n_tp)], axis=1)
         added = jnp.concatenate([mixed_s[j, here, :] for j in range(n_fs * n_tp)], axis=1)
         before = residual_scale * skip.astype(jnp.float32) + added.astype(jnp.float32)
         mid_s[here, :] = (normed(before) * mix_gain[...]).astype(jnp.bfloat16)
 
-    for copy in own_copies:
-        copy.wait()
-    weights_finish(0)
-    weights_finish(1)
-    keep = lax.broadcasted_iota(jnp.int32, (1, width), 1) + start_of(f) >= f * width
+    slot("f0")
+    for which in range(3):
+        sized(f, lambda size, which=which: own_copy(which, size).wait())
+    weight_finish(0)
+    weight_finish(1)
 
     for i in range(2):
         here = pl.ds(i * top, top)
         gate = jnp.dot(mid_s[here, :], gate_s[...], preferred_element_type=jnp.float32)
         upward = jnp.dot(mid_s[here, :], up_s[...], preferred_element_type=jnp.float32)
         value = gate / (1.0 + jnp.exp(-gate)) * upward
-        hid_s[here, :] = jnp.where(keep, value, 0.0).astype(jnp.bfloat16)
+        hid_s[here, :] = value.astype(jnp.bfloat16)
         if i == 0:
-            weights_forward(2, late)
-
-    weights_finish(2)
+            slot("f1")
+
+    weight_finish(2)
     span = down_s.shape[2]
-    per_half = n_fs // n_tp
+    per_core = n_fs // n_tp
 
     def project(side):
-        @pl.loop(0, per_half)
+        @pl.loop(0, per_core)
         def _(j):
             part_s[side, :, pl.ds(pl.multiple_of(j * span, span), span)] = jnp.dot(
-                hid_s[...], down_s[side * per_half + j], preferred_element_type=jnp.float32
+                hid_s[...], down_s[side * per_core + j], preferred_element_type=jnp.float32
             ).astype(jnp.bfloat16)
-
-    def rows_of(i):
-        return pl.ds(pl.multiple_of(i * length, length), length)
 
     def toward(step, low):
         return ((hi + step) % n_hi) * 2 + low
@@ -459,12 +606,11 @@
     average, second = stats[:, 0:1], stats[:, 1:2]
     scaled = (final - average) * lax.rsqrt(second - average * average + epsilon)
     out[...] = (scaled * out_gain[t]).astype(jnp.bfloat16)
-    for copy in pending:
-        copy.wait_send()
+    for wait in pending:
+        wait()
 
 
 def by_kernel(
-    width,
     tokens,
     lin_weight,
     glu_weight,
@@ -482,27 +628,22 @@
     rows, model = n_fs * length, feat * n_tp
     depth, own_chans = lin_weight.shape
     chans = own_chans // n_fs
-    n_taps = conv_taps.shape[0]
-    glu_mix = jnp.concatenate(
-        (
-            lin_weight.reshape(depth, n_fs, chans).transpose(1, 0, 2),
-            glu_weight.reshape(depth, n_fs, chans).transpose(1, 0, 2),
-        ),
-        axis=2,
-    )
-    own_taps = lax.dynamic_slice_in_dim(conv_taps, lax.axis_index("fs") * chans, chans, 1)
-    taps = jnp.concatenate((own_taps, own_taps), axis=1)
+    width, narrow = widths(ff_gate.shape[1], n_fs)
     vmem, far = pl.BlockSpec(memory_space=pltpu.VMEM), pl.BlockSpec(memory_space=pl.ANY)
     bf, fl = jnp.bfloat16, jnp.float32
     span = ff_down.shape[1]
     pair = lambda n: pltpu.SemaphoreType.DMA((2, n))
     result = pl.pallas_call(
-        functools.partial(fused, n_fs, n_tp, width),
+        functools.partial(fused, n_fs, n_tp, width, narrow),
         out_shape=jax.ShapeDtypeStruct((length, feat), bf),
-        in_specs=[vmem] * 6 + [far] * 3 + [vmem],
+        in_specs=[far] * 4 + [vmem] * 3 + [far] * 3 + [vmem],
         out_specs=vmem,
         scratch_shapes=[
             pltpu.VMEM((n_tp, rows, feat), bf),
+            pltpu.VMEM((depth, own_chans), bf),
+            pltpu.VMEM((depth, own_chans), bf),
+            pltpu.VMEM(conv_taps.shape, fl),
+            pltpu.VMEM((n_fs, depth, 2 * chans), bf),
             pltpu.VMEM((n_fs * depth, 2 * chans), bf),
             pltpu.VMEM((n_tp, 1, own_chans), fl),
             pltpu.VMEM((n_tp, own_chans, span // n_tp), bf),
@@ -520,7 +661,9 @@
             pltpu.VMEM((rows, feat), bf),
             pltpu.VMEM((rows, feat), bf),
             pltpu.VMEM((n_fs // 2, length, feat), bf),
+            pltpu.VMEM((n_fs // 2, length, feat), bf),
             pltpu.VMEM((n_tp, length, LANES), fl),
+            pair(n_fs),
             pair(n_fs),
             pair(3),
             pair(2 * n_fs),
@@ -528,20 +671,19 @@
             pair(2 * n_fs),
             pair(3 * n_fs),
             pair(3 * n_fs),
-            pltpu.SemaphoreType.DMA((6,)),
+            pltpu.SemaphoreType.DMA((7,)),
             pair(n_fs),
             pair(n_fs // 2),
-            pltpu.VMEM((n_fs // 2, length, feat), bf),
             pair(n_fs // 2),
-            pair(n_fs),
         ],
         compiler_params=pltpu.CompilerParams(
             collective_id=0, has_side_effects=True, vmem_limit_bytes=60 * 2**20
         ),
     )(
         tokens[0],
-        glu_mix,
-        taps,
+        lin_weight,
+        glu_weight,
+        conv_taps,
         conv_gain[None],
         conv_out_weight,
         mix_gain[None],
@@ -553,28 +695,35 @@
     return result[None]
 
 
+def widths(units, n_fs):
+    half = n_fs // 2
+    blocks = units // LANES // 2
+    most = -(-blocks // half)
+    return most * LANES, (blocks - most * (half - 1)) * LANES
+
+
 def on_device(*args):
     tokens, lin_weight, conv_out_weight, ff_gate = args[0], args[1], args[5], args[7]
     n_fs, n_tp, n_rep = (lax.axis_size(a) for a in ("fs", "tp", "rep"))
     seqs, length, feat = tokens.shape
     units = ff_gate.shape[1]
-    width = -(-units // (n_fs * LANES)) * LANES
+    width, narrow = widths(units, n_fs)
     fits = (
         n_rep == 2
         and n_tp == 2
-        and n_fs % 4 == 0
+        and n_fs == 8
         and seqs == 1
         and length % 16 == 0
         and args[3].shape[0] <= 33
         and lin_weight.shape[1] * 2 == n_fs * LANES
         and conv_out_weight.shape[1] == n_tp * LANES
         and feat % LANES == 0
-        and units % LANES == 0
-        and width * (n_fs - 1) < units
+        and units % (2 * LANES) == 0
+        and narrow == width - LANES > 0
         and lin_weight.shape[0] % 32 == 0
     )
     if fits:
-        return by_kernel(width, *args)
+        return by_kernel(*args)
     return by_collectives(*args)
 
 

time: 145 us -> 127 us (0.88)
  the two profiles are of different devices: /device:TPU:11 before, /device:TPU:23 now
where the time goes in v1:
time: 127 us; the launch traced here: 125 us
  Pallas kernels  124 us (98%)
  local copies, waits for them, and re-layouts  1.57 us (1%)
    pallas_call x1, Pallas kernels, by_kernel(): pl.pallas_call(functools.partial(fused, n_fs, n_tp, width, narrow), out_s...  124 us

profile of v1, /device:TPU:23, one launch (start us, length us, event | category | flops | bytes accessed | tf_op | source)
XLA Modules:
  0.0 125.3 jit_solution(13124635536219698361)
XLA Ops:
  0.0 123.7 %shard_map.109 = bf16[64,1024]{1,0:T(8,128)(2,1)} custom-call(bf16[64,1024]{1,0:T(8,128)(2,1)} %bitcast.6, bf16[256,512]{1,0:T(8,128)(2,1)} %lin_hbm.1, bf16[256,512]{1,0:T(8,128)(2,1)} %glu_hbm.1, f32[31,512]{1,0:T(8,128)} %taps_hbm.1, f32[1,512]{1,0:T(1,128)} %bitcast.9, bf16[512,256]{1,0:T(8,128)(2,1)} %out_weight.1, f32[1,2048]{1,0:T(1,128)} %bitcast.7, ...), custom_call_target="tpu_custom_call" | custom-call | tf_op jit(solution)/shard_map/pallas_call | solution.py:636
  123.7 1.6 %copy.13 = bf16[1,64,1024]{2,1,0:T(8,128)(2,1)} copy(bf16[1,64,1024]{2,1,0:T(8,128)(2,1)} %bitcast.5) | data formatting | bytes 262144

commit v2 on v1

--- a/solution.py
+++ b/solution.py
@@ -120,30 +120,48 @@
 NEAR = ((1, 0), (1, 1), (0, 1))
 OTHERS = FIRST + CROSS + NEAR
 G, U, D = 0, 1, 2
-SENDS = {
-    "t0": ((G, 2, 0),),
-    "t3": ((U, 2, 0),),
-    "t5": ((G, 3, 0), (G, 1, 0), (U, 3, 0)),
-    "t7": ((G, 0, 1),),
-    "c0": ((G, 2, 1),),
-    "c5": ((U, 2, 1), (U, 1, 0)),
-    "c7": ((G, 3, 1), (U, 0, 1), (G, 1, 1)),
-    "m0": ((U, 3, 1),),
-    "m3": ((U, 1, 1), (D, 2, 0)),
-    "m5": ((D, 3, 0),),
-    "m7": ((D, 2, 1), (D, 3, 1), (D, 1, 0), (D, 1, 1), (D, 0, 1)),
+INNER = {
+    "t0": ((1, G, 2, 0), (1, G, 3, 0),),
+    "t3": ((1, U, 2, 0),),
+    "t5": ((1, U, 3, 0), (1, G, 1, 0),),
+    "t6": ((1, G, 1, 1),),
+    "t7": ((1, G, 0, 1), (1, G, 2, 1),),
+    "c0": ((1, G, 3, 1),),
+    "c2": ((0, G, 3, 0), (1, U, 1, 0),),
+    "c3": ((1, U, 2, 1), (1, U, 3, 1),),
+    "c4": ((0, G, 2, 0), (0, U, 3, 0), (1, U, 1, 1),),
+    "c6": ((0, G, 1, 0), (0, U, 2, 0),),
+    "c7": ((1, U, 0, 1), (1, D, 2, 0), (0, G, 0, 1),),
+    "m0": ((1, D, 3, 0), (0, G, 3, 1), (0, G, 2, 1),),
+    "m1": ((0, U, 3, 1), (0, U, 2, 1),),
+    "m2": ((0, U, 1, 0), (0, U, 0, 1),),
+    "m3": ((0, G, 1, 1),),
+    "m4": ((1, D, 1, 0), (0, U, 1, 1),),
+    "m5": ((1, D, 2, 1), (1, D, 3, 1), (1, D, 1, 1),),
+    "m6": ((0, D, 2, 0),),
+    "m7": ((0, D, 3, 0), (1, D, 0, 1),),
+    "w2": ((0, D, 3, 1), (0, D, 2, 1),),
 }
-FORWARDS = {
-    "c0": ((G, 2, 0), (U, 2, 0)),
-    "c4": ((G, 3, 0),),
-    "c6": ((G, 1, 0), (U, 3, 0), (G, 0, 1)),
-    "m0": ((G, 2, 1),),
-    "m2": ((U, 2, 1), (U, 1, 0)),
-    "m4": ((G, 3, 1), (U, 0, 1)),
-    "m6": ((G, 1, 1), (U, 3, 1)),
-    "m8": ((U, 1, 1), (D, 2, 0)),
-    "f0": ((D, 3, 0),),
-    "f1": ((D, 2, 1), (D, 3, 1), (D, 1, 0), (D, 1, 1), (D, 0, 1)),
+OUTER = {
+    "t3": ((1, G, 2, 0), (1, G, 3, 0),),
+    "t5": ((1, U, 2, 0), (1, G, 1, 0),),
+    "t7": ((1, G, 0, 1),),
+    "c0": ((1, U, 3, 0),),
+    "c2": ((0, G, 2, 0),),
+    "c3": ((1, G, 2, 1), (1, G, 3, 1),),
+    "c4": ((0, U, 2, 0), (0, G, 3, 0), (0, G, 1, 0),),
+    "c5": ((1, U, 2, 1), (1, U, 3, 1),),
+    "c6": ((0, U, 3, 0), (0, G, 1, 1),),
+    "c7": ((1, U, 0, 1), (1, U, 1, 0), (1, G, 1, 1), (0, G, 0, 1),),
+    "m0": ((1, U, 1, 1), (0, G, 2, 1), (0, G, 3, 1),),
+    "m1": ((0, U, 2, 1),),
+    "m2": ((0, U, 3, 1),),
+    "m3": ((1, D, 2, 0), (0, U, 1, 0), (0, U, 0, 1),),
+    "m4": ((0, U, 1, 1),),
+    "m5": ((1, D, 3, 0), (1, D, 2, 1), (1, D, 3, 1),),
+    "m7": ((0, D, 2, 0), (1, D, 1, 0), (1, D, 1, 1), (1, D, 0, 1),),
+    "m8": ((0, D, 3, 0),),
+    "w2": ((0, D, 3, 1), (0, D, 2, 1),),
 }
 
 def fused(
@@ -180,11 +198,12 @@
     gate_s,
     up_s,
     down_s,
+    ff_s,
     hid_s,
     part_s,
     half_s,
     sum_s,
-    q_s,
+    z_s,
     y_s,
     stat_s,
     glu_sems,
@@ -197,7 +216,7 @@
     cross_sems,
     local_sems,
     half_sems,
-    q_sems,
+    z_sems,
     y_sems,
 ):
     rep, f, t = lax.axis_index("rep"), lax.axis_index("fs"), lax.axis_index("tp")
@@ -320,11 +339,16 @@
         send(block, block, sems, 3, beside)
         send(block, block, sems, 7, partner)
 
+    inner = (hi % n_hi) // (n_hi // 2) != hi % 2
+
     def slot(name):
-        for which, *k in SENDS.get(name, ()):
-            weight_send(which, tuple(k))
-        for which, *k in FORWARDS.get(name, ()):
-            weight_forward(which, tuple(k))
+        for role, table in ((inner, INNER), (jnp.logical_not(inner), OUTER)):
+            steps = table.get(name, ())
+
+            @pl.when(role)
+            def _(steps=steps):
+                for send_it, which, *k in steps:
+                    (weight_send if send_it else weight_forward)(which, tuple(k))
 
     def gather_finish(place, sems, name, between=None):
         between = between or {}
@@ -339,17 +363,17 @@
             receive(block, sems, index)
             return block
 
-        block = got(1, (1, 0))
-        send(block, block, sems, 4, beside)
-        send(block, block, sems, 7 + code((1, 0)), partner)
-        pause(1)
         block = got(3, (0, 1))
         send(block, block, sems, 7 + code((0, 1)), partner)
-        pause(2)
+        pause(1)
         block = got(0, (2, 0))
         send(block, block, sems, 2, close)
         send(block, block, sems, 5, beside)
         send(block, block, sems, 7 + code((2, 0)), partner)
+        pause(2)
+        block = got(1, (1, 0))
+        send(block, block, sems, 4, beside)
+        send(block, block, sems, 7 + code((1, 0)), partner)
         pause(3)
         block = got(4, (1, 1))
         send(block, block, sems, 7 + code((1, 1)), partner)
@@ -381,44 +405,43 @@
             (down_hbm.at[from_down], down_s.at[source, deep]),
         )[which]
 
+    def whole(which, k):
+        return which == D and k in NEAR
+
+    def weight_copy(which, k, size):
+        to = along(k)
+        if whole(which, k):
+            src, dst = down_hbm.at[pl.ds(start_of(to), size)], down_s.at[f, pl.ds(0, size)]
+        else:
+            src, dst = piece(which, to, f, rep, size)
+        return remote(src, dst, ff_sems, which * n_fs + code(k), (rep, to, t))
+
     def weight_send(which, k):
-        to = along(k)
-
-        def copy(size):
-            src, dst = piece(which, to, f, rep, size)
-            return remote(src, dst, ff_sems, which * n_fs + code(k), (rep, to, t))
-
-        sized(to, lambda size: copy(size).start())
-        pending.append(lambda: sized(to, lambda size: copy(size).wait_send()))
+        sized(along(k), lambda size: weight_copy(which, k, size).start())
+
+    def cross_copy(which, k, size):
+        block = piece(which, f, along(k), rep, size)[1]
+        return remote(block, block, cross_sems, which * n_fs + code(k), mirror)
 
     def weight_forward(which, k):
-        index = which * n_fs + code(k)
-
-        def block(size):
-            return piece(which, f, along(k), rep, size)[1]
-
         def action(size):
-            receive(block(size), ff_sems, index)
-            remote(block(size), block(size), cross_sems, index, mirror).start()
+            block = piece(which, f, along(k), rep, size)[1]
+            receive(block, ff_sems, which * n_fs + code(k))
+            cross_copy(which, k, size).start()
 
         sized(f, action)
-        pending.append(
-            lambda: sized(
-                f,
-                lambda size: remote(
-                    block(size), block(size), cross_sems, index, mirror
-                ).wait_send(),
-            )
-        )
-
-    def weight_finish(which):
-        for k in OTHERS:
-            sized(
-                f,
-                lambda size: receive(
-                    piece(which, f, along(k), 1 - rep, size)[1], cross_sems, which * n_fs + code(k)
-                ),
-            )
+
+    def weight_finish(which, ks):
+        for k in ks:
+            index = which * n_fs + code(k)
+
+            def action(size):
+                if whole(which, k):
+                    receive(down_s.at[along(k), pl.ds(0, size)], ff_sems, index)
+                else:
+                    receive(piece(which, f, along(k), 1 - rep, size)[1], cross_sems, index)
+
+            sized(f, action)
 
     pl.semaphore_wait(barrier, n_fs + 1)
     fetches[0].wait()
@@ -483,6 +506,7 @@
     taps = jnp.where((lanes < chans) == (f % 2 == 0), tap_pair, turned)
     n_taps = taps.shape[0]
     margin = (n_taps - 1) // 2
+    slot("d0")
     conv_slot = lambda i, j: conv_s.at[j * n_fs + i]
     groups = n_fs // 2
     for g in range(groups):
@@ -513,6 +537,7 @@
         v = normed(norm_s[here, :]) * gains
         act_s[here, :] = (v / (1.0 + jnp.exp(-v))).astype(jnp.bfloat16)
 
+    slot("n0")
     share = proj_s.shape[1]
     mixed_slot = lambda i, j: mixed_s.at[i * n_tp + j]
     mixed_s[f * n_tp + t] = sum(
@@ -536,24 +561,39 @@
         before = residual_scale * skip.astype(jnp.float32) + added.astype(jnp.float32)
         mid_s[here, :] = (normed(before) * mix_gain[...]).astype(jnp.bfloat16)
 
-    slot("f0")
-    for which in range(3):
-        sized(f, lambda size, which=which: own_copy(which, size).wait())
-    weight_finish(0)
-    weight_finish(1)
-
-    for i in range(2):
-        here = pl.ds(i * top, top)
-        gate = jnp.dot(mid_s[here, :], gate_s[...], preferred_element_type=jnp.float32)
-        upward = jnp.dot(mid_s[here, :], up_s[...], preferred_element_type=jnp.float32)
-        value = gate / (1.0 + jnp.exp(-gate)) * upward
-        hid_s[here, :] = value.astype(jnp.bfloat16)
-        if i == 0:
-            slot("f1")
-
-    weight_finish(2)
+    slot("e0")
+    near_side = hi // (n_hi // 2)
+    deep = n_fs // n_tp * depth
+
+    def partial_ff(side):
+        inner_rows = pl.ds(pl.multiple_of(side * deep, deep), deep)
+        left = mid_s[:, inner_rows]
+        return tuple(
+            jnp.dot(left, right[inner_rows, :], preferred_element_type=jnp.float32)
+            for right in (gate_s, up_s)
+        )
+
+    for which in (0, 1):
+        sized(f, lambda size: own_copy(which, size).wait())
+        weight_finish(which, NEAR)
+        slot("w" + str(which))
+    ff_s[0], ff_s[1] = partial_ff(near_side)
+    slot("w2")
+    for i, (which, ks) in enumerate(((0, FIRST), (1, FIRST), (0, CROSS), (1, CROSS))):
+        weight_finish(which, ks)
+        slot("w" + str(3 + i))
+
+    gate, upward = partial_ff(1 - near_side)
+    gate, upward = gate + ff_s[0], upward + ff_s[1]
+    hid_s[...] = (gate / (1.0 + jnp.exp(-gate)) * upward).astype(jnp.bfloat16)
+    slot("g0")
+
+    sized(f, lambda size: own_copy(2, size).wait())
+    weight_finish(2, NEAR)
+    slot("g2")
     span = down_s.shape[2]
     per_core = n_fs // n_tp
+    steps = (3, 2, 1, 0)
 
     def project(side):
         @pl.loop(0, per_core)
@@ -562,35 +602,56 @@
                 hid_s[...], down_s[side * per_core + j], preferred_element_type=jnp.float32
             ).astype(jnp.bfloat16)
 
-    def toward(step, low):
-        return ((hi + step) % n_hi) * 2 + low
-
-    steps = list(range(1, n_hi)) + [0]
-    project(other)
+    def half_copy(k):
+        here = rows_of(along(k))
+        return remote(part_s.at[other, here], half_s.at[here], half_sems, code(k), partner)
+
+    def hand_over():
+        for low in (1, 0):
+            for d in steps:
+                half_copy((d, low)).start()
+
+    def joined(k):
+        here = rows_of(along(k))
+        receive(half_s.at[here], half_sems, code(k))
+        return part_s[t, here, :].astype(jnp.float32) + half_s[here, :].astype(jnp.float32)
+
+    def aside_copy(d):
+        return remote(sum_s.at[rows_of(along((d, 1)))], y_s.at[d], y_sems, d, beside)
+
+    def aside():
+        for d in steps:
+            sum_s[rows_of(along((d, 1))), :] = joined((d, 1)).astype(jnp.bfloat16)
+            aside_copy(d).start()
+
+    project(near_side)
+    pl.when(t == near_side)(aside)
+    pl.when(t != near_side)(hand_over)
+    slot("g3")
+    weight_finish(2, FIRST + CROSS)
+    project(1 - near_side)
+    pl.when(t == near_side)(hand_over)
+    pl.when(t != near_side)(aside)
     for d in steps:
-        for e, low in enumerate((1 - lo, lo)):
-            here = rows_of(toward(d, low))
-            send(part_s.at[other, here], half_s.at[here], half_sems, 2 * d + e, partner)
-    project(t)
+        pending.append(aside_copy(d).wait_send)
+        for low in (0, 1):
+            pending.append(half_copy((d, low)).wait_send)
+
     for d in steps:
-        here = rows_of(toward(d, 1 - lo))
-        receive(half_s.at[here], half_sems, 2 * d)
-        both = part_s[t, here, :].astype(jnp.float32) + half_s[here, :].astype(jnp.float32)
-        sum_s[here, :] = both.astype(jnp.bfloat16)
-        send(sum_s.at[here], y_s.at[d], y_sems, d, (rep, hi * 2 + 1 - lo, t))
-    for d in steps:
-        to = toward(d, lo)
-        here = rows_of(to)
-        receive(half_s.at[here], half_sems, 2 * d + 1)
-        both = part_s[t, here, :].astype(jnp.float32) + half_s[here, :].astype(jnp.float32)
+        here = rows_of(along((d, 0)))
+        forward = joined((d, 0))
         receive(y_s.at[d], y_sems, d)
-        forward = both + y_s[d].astype(jnp.float32)
-        if d:
+        forward = forward + y_s[d].astype(jnp.float32)
+        if d % 2:
             sum_s[here, :] = forward.astype(jnp.bfloat16)
-            send(sum_s.at[here], q_s.at[d], q_sems, d, (rep, to, t))
-    for d in range(1, n_hi):
-        receive(q_s.at[d], q_sems, d)
-        forward = forward + q_s[d].astype(jnp.float32)
+            send(sum_s.at[here], z_s.at[d // 2], z_sems, d // 2, close)
+        elif d:
+            receive(z_s.at[1], z_sems, 1)
+            sum_s[here, :] = (forward + z_s[1].astype(jnp.float32)).astype(jnp.bfloat16)
+            send(sum_s.at[here], z_s.at[2], z_sems, 2, far)
+    for i in (0, 2):
+        receive(z_s.at[i], z_sems, i)
+        forward = forward + z_s[i].astype(jnp.float32)
     forward = forward.astype(jnp.bfloat16).astype(jnp.float32)
     own_half = pl.ds(pl.multiple_of(t * feat, feat), feat)
     final = residual_scale * mid_s[rows_of(f), own_half].astype(jnp.float32) + forward
@@ -608,6 +669,11 @@
     out[...] = (scaled * out_gain[t]).astype(jnp.bfloat16)
     for wait in pending:
         wait()
+    for which in range(3):
+        for k in OTHERS:
+            sized(along(k), lambda size: weight_copy(which, k, size).wait_send())
+            if not whole(which, k):
+                sized(f, lambda size: cross_copy(which, k, size).wait_send())
 
 
 def by_kernel(
@@ -656,11 +722,12 @@
             pltpu.VMEM((n_fs * depth, width), bf),
             pltpu.VMEM((n_fs * depth, width), bf),
             pltpu.VMEM((n_fs, width, span), bf),
+            pltpu.VMEM((2, rows, width), fl),
             pltpu.VMEM((rows, width), bf),
             pltpu.VMEM((n_tp, rows, feat), bf),
             pltpu.VMEM((rows, feat), bf),
             pltpu.VMEM((rows, feat), bf),
-            pltpu.VMEM((n_fs // 2, length, feat), bf),
+            pltpu.VMEM((3, length, feat), bf),
             pltpu.VMEM((n_fs // 2, length, feat), bf),
             pltpu.VMEM((n_tp, length, LANES), fl),
             pair(n_fs),
@@ -673,7 +740,7 @@
             pair(3 * n_fs),
             pltpu.SemaphoreType.DMA((7,)),
             pair(n_fs),
-            pair(n_fs // 2),
+            pair(3),
             pair(n_fs // 2),
         ],
         compiler_params=pltpu.CompilerParams(

time: 127 us -> 116 us (0.913)
  Pallas kernels: 124 us -> 113 us
    pallas_call x1, Pallas kernels: 124 us -> 113 us  [by_kernel(): pl.pallas_call(functools.partial(fused, n_fs, n_tp, width, narrow), out_s...]
where the time goes in v2:
time: 116 us; the launch traced here: 114 us
  Pallas kernels  113 us (97%)
  local copies, waits for them, and re-layouts  1.57 us (1%)
    pallas_call x1, Pallas kernels, by_kernel(): pl.pallas_call(functools.partial(fused, n_fs, n_tp, width, narrow), out_s...  113 us

profile of v2, /device:TPU:23, one launch (start us, length us, event | category | flops | bytes accessed | tf_op | source)
XLA Modules:
  0.0 114.4 jit_solution(5030796578083245203)
XLA Ops:
  0.0 112.8 %shard_map.109 = bf16[64,1024]{1,0:T(8,128)(2,1)} custom-call(bf16[64,1024]{1,0:T(8,128)(2,1)} %bitcast.6, bf16[256,512]{1,0:T(8,128)(2,1)} %lin_hbm.1, bf16[256,512]{1,0:T(8,128)(2,1)} %glu_hbm.1, f32[31,512]{1,0:T(8,128)} %taps_hbm.1, f32[1,512]{1,0:T(1,128)} %bitcast.9, bf16[512,256]{1,0:T(8,128)(2,1)} %out_weight.1, f32[1,2048]{1,0:T(1,128)} %bitcast.7, ...), custom_call_target="tpu_custom_call" | custom-call | tf_op jit(solution)/shard_map/pallas_call | solution.py:702
  112.8 1.6 %copy.13 = bf16[1,64,1024]{2,1,0:T(8,128)(2,1)} copy(bf16[1,64,1024]{2,1,0:T(8,128)(2,1)} %bitcast.5) | data formatting | bytes 262144

commit v3 on v2

--- a/solution.py
+++ b/solution.py
@@ -121,11 +121,11 @@
 OTHERS = FIRST + CROSS + NEAR
 G, U, D = 0, 1, 2
 INNER = {
-    "t0": ((1, G, 2, 0), (1, G, 3, 0),),
+    "t0": ((1, G, 2, 0), (1, G, 3, 0), (1, G, 0, 1),),
     "t3": ((1, U, 2, 0),),
     "t5": ((1, U, 3, 0), (1, G, 1, 0),),
     "t6": ((1, G, 1, 1),),
-    "t7": ((1, G, 0, 1), (1, G, 2, 1),),
+    "t7": ((1, G, 2, 1), (1, D, 0, 1),),
     "c0": ((1, G, 3, 1),),
     "c2": ((0, G, 3, 0), (1, U, 1, 0),),
     "c3": ((1, U, 2, 1), (1, U, 3, 1),),
@@ -139,13 +139,13 @@
     "m4": ((1, D, 1, 0), (0, U, 1, 1),),
     "m5": ((1, D, 2, 1), (1, D, 3, 1), (1, D, 1, 1),),
     "m6": ((0, D, 2, 0),),
-    "m7": ((0, D, 3, 0), (1, D, 0, 1),),
+    "m7": ((0, D, 3, 0),),
     "w2": ((0, D, 3, 1), (0, D, 2, 1),),
 }
 OUTER = {
     "t3": ((1, G, 2, 0), (1, G, 3, 0),),
     "t5": ((1, U, 2, 0), (1, G, 1, 0),),
-    "t7": ((1, G, 0, 1),),
+    "t7": ((1, D, 0, 1),),
     "c0": ((1, U, 3, 0),),
     "c2": ((0, G, 2, 0),),
     "c3": ((1, G, 2, 1), (1, G, 3, 1),),
@@ -159,9 +159,10 @@
     "m3": ((1, D, 2, 0), (0, U, 1, 0), (0, U, 0, 1),),
     "m4": ((0, U, 1, 1),),
     "m5": ((1, D, 3, 0), (1, D, 2, 1), (1, D, 3, 1),),
-    "m7": ((0, D, 2, 0), (1, D, 1, 0), (1, D, 1, 1), (1, D, 0, 1),),
+    "m7": ((0, D, 2, 0), (1, D, 1, 0), (1, D, 1, 1),),
     "m8": ((0, D, 3, 0),),
     "w2": ((0, D, 3, 1), (0, D, 2, 1),),
+    "t0": ((1, G, 0, 1),),
 }
 
 def fused(
@@ -206,6 +207,7 @@
     z_s,
     y_s,
     stat_s,
+    out_s,
     glu_sems,
     glu_cross_sems,
     small_sems,
@@ -229,7 +231,6 @@
     depth = gate_hbm.shape[0]
     half_depth = depth // 2
     chans = LANES // 2
-    pending = []
 
     def flip(z, step):
         return z + step - 2 * step * ((z // step) % 2)
@@ -308,20 +309,18 @@
         up_s[:, narrow:] = jnp.zeros((n_fs * depth, width - narrow), jnp.bfloat16)
         down_s[:, narrow:, :] = jnp.zeros((n_fs, width - narrow, down_s.shape[2]), jnp.bfloat16)
 
-    def remote(src, dst, sems, index, device):
+    def remote(src, dst, send_sem, recv_sem, device):
         return pltpu.make_async_remote_copy(
             src_ref=src,
             dst_ref=dst,
-            send_sem=sems.at[0, index],
-            recv_sem=sems.at[1, index],
+            send_sem=send_sem,
+            recv_sem=recv_sem,
             device_id=device,
             device_id_type=MESH,
         )
 
-    def send(*parts):
-        copy = remote(*parts)
-        copy.start()
-        pending.append(copy.wait_send)
+    def send(src, dst, sems, index, device):
+        remote(src, dst, sems.at[0], sems.at[1 + index], device).start()
 
     partner = (rep, f, other)
     mirror = (1 - rep, f, t)
@@ -329,8 +328,17 @@
     close = (rep, along((1, 0)), t)
     far = (rep, along((2, 0)), t)
 
+    def arrive(dst, sem):
+        remote(dst, dst, sem, sem, partner).wait_recv()
+
     def receive(dst, sems, index):
-        remote(dst, dst, sems, index, partner).wait_recv()
+        arrive(dst, sems.at[1 + index])
+
+    def sent(src, sem):
+        remote(src, src, sem, sem, partner).wait_send()
+
+    def small_copy(src, dst, index):
+        return remote(src, dst, small_sems.at[index], small_sems.at[3 + index], partner)
 
     def gather_start(slot, sems):
         block = slot(f, t)
@@ -350,7 +358,7 @@
                 for send_it, which, *k in steps:
                     (weight_send if send_it else weight_forward)(which, tuple(k))
 
-    def gather_finish(place, sems, name, between=None):
+    def gather_finish(place, all_of, sems, name, between=None):
         between = between or {}
 
         def pause(step):
@@ -364,32 +372,31 @@
             return block
 
         block = got(3, (0, 1))
-        send(block, block, sems, 7 + code((0, 1)), partner)
+        send(block, block, sems, 7, partner)
         pause(1)
         block = got(0, (2, 0))
         send(block, block, sems, 2, close)
         send(block, block, sems, 5, beside)
-        send(block, block, sems, 7 + code((2, 0)), partner)
+        send(block, block, sems, 7, partner)
         pause(2)
         block = got(1, (1, 0))
         send(block, block, sems, 4, beside)
-        send(block, block, sems, 7 + code((1, 0)), partner)
+        send(block, block, sems, 7, partner)
         pause(3)
         block = got(4, (1, 1))
-        send(block, block, sems, 7 + code((1, 1)), partner)
+        send(block, block, sems, 7, partner)
         pause(4)
         block = got(2, (3, 0))
         send(block, block, sems, 6, beside)
-        send(block, block, sems, 7 + code((3, 0)), partner)
+        send(block, block, sems, 7, partner)
         pause(5)
         block = got(5, (2, 1))
-        send(block, block, sems, 7 + code((2, 1)), partner)
+        send(block, block, sems, 7, partner)
         pause(6)
         block = got(6, (3, 1))
-        send(block, block, sems, 7 + code((3, 1)), partner)
+        send(block, block, sems, 7, partner)
         pause(7)
-        for k in ((0, 0),) + OTHERS:
-            receive(place(along(k), other), sems, 7 + code(k))
+        receive(all_of(other), sems, 7)
 
     half_width = width // 2
 
@@ -414,34 +421,41 @@
             src, dst = down_hbm.at[pl.ds(start_of(to), size)], down_s.at[f, pl.ds(0, size)]
         else:
             src, dst = piece(which, to, f, rep, size)
-        return remote(src, dst, ff_sems, which * n_fs + code(k), (rep, to, t))
+        return remote(
+            src, dst, ff_sems.at[3 * n_fs + code(k)], ff_sems.at[which * n_fs + code(k)], (rep, to, t)
+        )
 
     def weight_send(which, k):
         sized(along(k), lambda size: weight_copy(which, k, size).start())
 
+    def group_sem(which, k):
+        group = 0 if k in NEAR else 1 if k in FIRST else 2
+        return cross_sems.at[2 + (6 if which == D else 3 * which + group)]
+
     def cross_copy(which, k, size):
         block = piece(which, f, along(k), rep, size)[1]
-        return remote(block, block, cross_sems, which * n_fs + code(k), mirror)
+        return remote(block, block, cross_sems.at[which // 2], group_sem(which, k), mirror)
 
     def weight_forward(which, k):
         def action(size):
             block = piece(which, f, along(k), rep, size)[1]
-            receive(block, ff_sems, which * n_fs + code(k))
+            arrive(block, ff_sems.at[which * n_fs + code(k)])
             cross_copy(which, k, size).start()
 
         sized(f, action)
 
     def weight_finish(which, ks):
-        for k in ks:
-            index = which * n_fs + code(k)
-
-            def action(size):
-                if whole(which, k):
-                    receive(down_s.at[along(k), pl.ds(0, size)], ff_sems, index)
-                else:
-                    receive(piece(which, f, along(k), 1 - rep, size)[1], cross_sems, index)
-
-            sized(f, action)
+        def action(size):
+            if whole(which, ks[0]):
+                for k in ks:
+                    arrive(down_s.at[along(k), pl.ds(0, size)], ff_sems.at[which * n_fs + code(k)])
+            else:
+                arrive(
+                    gate_s.at[pl.ds(0, len(ks) * half_depth), pl.ds(0, size)],
+                    group_sem(which, ks[0]),
+                )
+
+        sized(f, action)
 
     pl.semaphore_wait(barrier, n_fs + 1)
     fetches[0].wait()
@@ -462,8 +476,8 @@
     slot("t0")
     columns = pl.ds(pl.multiple_of(other * LANES, LANES), LANES)
     own_columns = pl.ds(pl.multiple_of(t * LANES, LANES), LANES)
-    send(gain, gain_s.at[t], small_sems, 0, partner)
-    send(out_weight.at[:, columns], proj_s.at[t], small_sems, 1, partner)
+    small_copy(gain, gain_s.at[t], 0).start()
+    small_copy(out_weight.at[:, columns], proj_s.at[t], 1).start()
 
     glu_s[pl.ds(pl.multiple_of(f * depth, depth), depth), :] = mix_s[f]
     gain_s[t] = gain[...]
@@ -474,10 +488,11 @@
         for k in ks:
             block = glu_piece(along(k), rep)
             receive(block, glu_sems, code(k))
-            send(block, block, glu_cross_sems, code(k), mirror)
+            send(block, block, glu_cross_sems, 0, mirror)
 
     gather_finish(
         tok_slot,
+        lambda j: x_s.at[j],
         tok_sems,
         "t",
         {
@@ -486,8 +501,8 @@
             6: lambda: glu_forward(CROSS),
         },
     )
-    for k in OTHERS:
-        receive(glu_piece(along(k), 1 - rep), glu_cross_sems, code(k))
+    seven = glu_s.at[pl.ds(0, len(OTHERS) * half_depth)]
+    receive(seven, glu_cross_sems, 0)
 
     product = sum(
         jnp.dot(
@@ -519,9 +534,11 @@
         conv_s[t * n_fs + f, g * length : (g + 1) * length, :] = acc.astype(jnp.bfloat16)
     gather_start(conv_slot, conv_sems)
     slot("c0")
-    gather_finish(conv_slot, conv_sems, "c")
-    receive(gain_s.at[other], small_sems, 0)
-    receive(proj_s.at[other], small_sems, 1)
+    gather_finish(
+        conv_slot, lambda j: conv_s.at[pl.ds(j * n_fs, n_fs)], conv_sems, "c"
+    )
+    small_copy(gain_s.at[other], gain_s.at[other], 0).wait_recv()
+    small_copy(proj_s.at[other], proj_s.at[other], 1).wait_recv()
 
     for j in range(n_fs * n_tp // 2):
         left = conv_s[2 * j].astype(jnp.float32)
@@ -539,8 +556,8 @@
 
     slot("n0")
     share = proj_s.shape[1]
-    mixed_slot = lambda i, j: mixed_s.at[i * n_tp + j]
-    mixed_s[f * n_tp + t] = sum(
+    mixed_slot = lambda i, j: mixed_s.at[j * n_fs + i]
+    mixed_s[t * n_fs + f] = sum(
         jnp.dot(
             act_s[:, j * share : (j + 1) * share],
             proj_s[j],
@@ -550,14 +567,18 @@
     ).astype(jnp.bfloat16)
     gather_start(mixed_slot, mixed_sems)
     slot("m0")
-    gather_finish(mixed_slot, mixed_sems, "m")
+    gather_finish(
+        mixed_slot, lambda j: mixed_s.at[pl.ds(j * n_fs, n_fs)], mixed_sems, "m"
+    )
     slot("m8")
 
     @pl.loop(0, n_fs)
     def _(i):
         here = rows_of(i)
         skip = jnp.concatenate([x_s[j, here, :] for j in range(n_tp)], axis=1)
-        added = jnp.concatenate([mixed_s[j, here, :] for j in range(n_fs * n_tp)], axis=1)
+        added = jnp.concatenate(
+            [mixed_s[j * n_fs + k, here, :] for k in range(n_fs) for j in range(n_tp)], axis=1
+        )
         before = residual_scale * skip.astype(jnp.float32) + added.astype(jnp.float32)
         mid_s[here, :] = (normed(before) * mix_gain[...]).astype(jnp.bfloat16)
 
@@ -604,7 +625,13 @@
 
     def half_copy(k):
         here = rows_of(along(k))
-        return remote(part_s.at[other, here], half_s.at[here], half_sems, code(k), partner)
+        return remote(
+            part_s.at[other, here],
+            half_s.at[here],
+            half_sems.at[0],
+            half_sems.at[1 + code(k)],
+            partner,
+        )
 
     def hand_over():
         for low in (1, 0):
@@ -617,7 +644,9 @@
         return part_s[t, here, :].astype(jnp.float32) + half_s[here, :].astype(jnp.float32)
 
     def aside_copy(d):
-        return remote(sum_s.at[rows_of(along((d, 1)))], y_s.at[d], y_sems, d, beside)
+        return remote(
+            sum_s.at[rows_of(along((d, 1)))], y_s.at[d], y_sems.at[0], y_sems.at[1 + d], beside
+        )
 
     def aside():
         for d in steps:
@@ -632,10 +661,6 @@
     project(1 - near_side)
     pl.when(t == near_side)(hand_over)
     pl.when(t != near_side)(aside)
-    for d in steps:
-        pending.append(aside_copy(d).wait_send)
-        for low in (0, 1):
-            pending.append(half_copy((d, low)).wait_send)
 
     for d in steps:
         here = rows_of(along((d, 0)))
@@ -661,19 +686,42 @@
         jnp.sum(final, axis=1, keepdims=True),
         jnp.sum(final * final, axis=1, keepdims=True),
     )
-    send(stat_s.at[t], stat_s.at[t], small_sems, 2, partner)
-    receive(stat_s.at[other], small_sems, 2)
+    small_copy(stat_s.at[t], stat_s.at[t], 2).start()
+    small_copy(stat_s.at[other], stat_s.at[other], 2).wait_recv()
     stats = (stat_s[0] + stat_s[1]) / model
     average, second = stats[:, 0:1], stats[:, 1:2]
     scaled = (final - average) * lax.rsqrt(second - average * average + epsilon)
-    out[...] = (scaled * out_gain[t]).astype(jnp.bfloat16)
-    for wait in pending:
-        wait()
-    for which in range(3):
-        for k in OTHERS:
-            sized(along(k), lambda size: weight_copy(which, k, size).wait_send())
-            if not whole(which, k):
-                sized(f, lambda size: cross_copy(which, k, size).wait_send())
+    out_s[...] = (scaled * out_gain[t]).astype(jnp.bfloat16)
+    result = pltpu.make_async_copy(out_s, out.at[0], local_sems.at[7])
+    result.start()
+    result.wait()
+    blocks = n_fs * n_tp - 1
+    sent(mixed_s.at[pl.ds(0, blocks)], tok_sems.at[0])
+    sent(conv_s.at[pl.ds(0, blocks)], conv_sems.at[0])
+    sent(mixed_s.at[pl.ds(0, blocks)], mixed_sems.at[0])
+    sent(seven, glu_sems.at[0])
+    sent(seven, glu_cross_sems.at[0])
+    sent(half_s, half_sems.at[0])
+    sent(y_s, y_sems.at[0])
+    sent(z_s, z_sems.at[0])
+    small_copy(gain, gain_s.at[t], 0).wait_send()
+    small_copy(out_weight.at[:, columns], proj_s.at[t], 1).wait_send()
+    small_copy(stat_s.at[t], stat_s.at[t], 2).wait_send()
+    for k in OTHERS:
+        deep_rows = pl.ds(0, (4 if k in NEAR else 3) * half_depth)
+        sized(
+            along(k),
+            lambda size: sent(
+                gate_s.at[deep_rows, pl.ds(0, size)], ff_sems.at[3 * n_fs + code(k)]
+            ),
+        )
+    for i, count in enumerate((2 * len(OTHERS), len(FIRST + CROSS))):
+        sized(
+            f,
+            lambda size: sent(
+                gate_s.at[pl.ds(0, count * half_depth), pl.ds(0, size)], cross_sems.at[i]
+            ),
+        )
 
 
 def by_kernel(
@@ -698,12 +746,12 @@
     vmem, far = pl.BlockSpec(memory_space=pltpu.VMEM), pl.BlockSpec(memory_space=pl.ANY)
     bf, fl = jnp.bfloat16, jnp.float32
     span = ff_down.shape[1]
-    pair = lambda n: pltpu.SemaphoreType.DMA((2, n))
+    dma = lambda n: pltpu.SemaphoreType.DMA((n,))
     result = pl.pallas_call(
         functools.partial(fused, n_fs, n_tp, width, narrow),
-        out_shape=jax.ShapeDtypeStruct((length, feat), bf),
+        out_shape=jax.ShapeDtypeStruct((1, length, feat), bf),
         in_specs=[far] * 4 + [vmem] * 3 + [far] * 3 + [vmem],
-        out_specs=vmem,
+        out_specs=far,
         scratch_shapes=[
             pltpu.VMEM((n_tp, rows, feat), bf),
             pltpu.VMEM((depth, own_chans), bf),
@@ -730,18 +778,19 @@
             pltpu.VMEM((3, length, feat), bf),
             pltpu.VMEM((n_fs // 2, length, feat), bf),
             pltpu.VMEM((n_tp, length, LANES), fl),
-            pair(n_fs),
-            pair(n_fs),
-            pair(3),
-            pair(2 * n_fs),
-            pair(2 * n_fs),
-            pair(2 * n_fs),
-            pair(3 * n_fs),
-            pair(3 * n_fs),
-            pltpu.SemaphoreType.DMA((7,)),
-            pair(n_fs),
-            pair(3),
-            pair(n_fs // 2),
+            pltpu.VMEM((length, feat), bf),
+            dma(n_fs + 1),
+            dma(2),
+            dma(6),
+            dma(n_fs + 1),
+            dma(n_fs + 1),
+            dma(n_fs + 1),
+            dma(4 * n_fs),
+            dma(9),
+            dma(8),
+            dma(n_fs + 1),
+            dma(4),
+            dma(n_fs // 2 + 1),
         ],
         compiler_params=pltpu.CompilerParams(
             collective_id=0, has_side_effects=True, vmem_limit_bytes=60 * 2**20
@@ -759,7 +808,7 @@
         ff_down,
         out_gain.reshape(n_tp, 1, feat),
     )
-    return result[None]
+    return result
 
 
 def widths(units, n_fs):

time: 116 us -> 113 us (0.974); the launches traced: 114 us -> 113 us
  Pallas kernels: 113 us -> 111 us
    pallas_call x1, Pallas kernels: 113 us -> 111 us  [by_kernel(): pl.pallas_call(functools.partial(fused, n_fs, n_tp, width, narrow), out_s...]
where the time goes in v3:
time: 113 us
  Pallas kernels  111 us (98%)
  local copies, waits for them, and re-layouts  1.57 us (1%)
    pallas_call x1, Pallas kernels, by_kernel(): pl.pallas_call(functools.partial(fused, n_fs, n_tp, width, narrow), out_s...  111 us

profile of v3, /device:TPU:23, one launch (start us, length us, event | category | flops | bytes accessed | tf_op | source)
XLA Modules:
  0.0 112.8 jit_solution(17850424874909130725)
XLA Ops:
  0.0 111.3 %shard_map.109 = bf16[1,64,1024]{2,1,0:T(8,128)(2,1)} custom-call(bf16[64,1024]{1,0:T(8,128)(2,1)} %bitcast.4, bf16[256,512]{1,0:T(8,128)(2,1)} %lin_hbm.1, bf16[256,512]{1,0:T(8,128)(2,1)} %glu_hbm.1, f32[31,512]{1,0:T(8,128)} %taps_hbm.1, f32[1,512]{1,0:T(1,128)} %bitcast.7, bf16[512,256]{1,0:T(8,128)(2,1)} %out_weight.1, f32[1,2048]{1,0:T(1,128)} %bitcast.5, ...), custom_call_target="tpu_custom_call" | custom-call | tf_op jit(solution)/shard_map/pallas_call | solution.py:750
  111.3 1.6 %copy.13 = bf16[1,64,1024]{2,1,0:T(8,128)(2,1)} copy(bf16[1,64,1024]{2,1,0:T(8,128)(2,1)} %shard_map.109) | data formatting | bytes 262144

commit v4 on v3

--- a/solution.py
+++ b/solution.py
@@ -623,35 +623,46 @@
                 hid_s[...], down_s[side * per_core + j], preferred_element_type=jnp.float32
             ).astype(jnp.bfloat16)
 
-    def half_copy(k):
+    pieces_of = tuple((d, h) for d in steps for h in (0, 1))
+
+    def cols(h):
+        return pl.ds(h * (feat // 2), feat // 2)
+
+    def half_copy(k, h):
         here = rows_of(along(k))
         return remote(
-            part_s.at[other, here],
-            half_s.at[here],
+            part_s.at[other, here, cols(h)],
+            half_s.at[here, cols(h)],
             half_sems.at[0],
-            half_sems.at[1 + code(k)],
+            half_sems.at[1 + 2 * code(k) + h],
             partner,
         )
 
     def hand_over():
         for low in (1, 0):
-            for d in steps:
-                half_copy((d, low)).start()
-
-    def joined(k):
+            for d, h in pieces_of:
+                half_copy((d, low), h).start()
+
+    def joined(k, h):
         here = rows_of(along(k))
-        receive(half_s.at[here], half_sems, code(k))
-        return part_s[t, here, :].astype(jnp.float32) + half_s[here, :].astype(jnp.float32)
-
-    def aside_copy(d):
+        receive(half_s.at[here, cols(h)], half_sems, 2 * code(k) + h)
+        return part_s[t, here, cols(h)].astype(jnp.float32) + half_s[here, cols(h)].astype(
+            jnp.float32
+        )
+
+    def aside_copy(d, h):
         return remote(
-            sum_s.at[rows_of(along((d, 1)))], y_s.at[d], y_sems.at[0], y_sems.at[1 + d], beside
+            sum_s.at[rows_of(along((d, 1))), cols(h)],
+            y_s.at[d, :, cols(h)],
+            y_sems.at[0],
+            y_sems.at[1 + 2 * d + h],
+            beside,
         )
 
     def aside():
-        for d in steps:
-            sum_s[rows_of(along((d, 1))), :] = joined((d, 1)).astype(jnp.bfloat16)
-            aside_copy(d).start()
+        for d, h in pieces_of:
+            sum_s[rows_of(along((d, 1))), cols(h)] = joined((d, 1), h).astype(jnp.bfloat16)
+            aside_copy(d, h).start()
 
     project(near_side)
     pl.when(t == near_side)(aside)
@@ -662,21 +673,35 @@
     pl.when(t == near_side)(hand_over)
     pl.when(t != near_side)(aside)
 
-    for d in steps:
+    def z_part(i, h):
+        return z_s.at[i, :, cols(h)]
+
+    ends = []
+    for d, h in pieces_of:
         here = rows_of(along((d, 0)))
-        forward = joined((d, 0))
-        receive(y_s.at[d], y_sems, d)
-        forward = forward + y_s[d].astype(jnp.float32)
-        if d % 2:
-            sum_s[here, :] = forward.astype(jnp.bfloat16)
-            send(sum_s.at[here], z_s.at[d // 2], z_sems, d // 2, close)
-        elif d:
-            receive(z_s.at[1], z_sems, 1)
-            sum_s[here, :] = (forward + z_s[1].astype(jnp.float32)).astype(jnp.bfloat16)
-            send(sum_s.at[here], z_s.at[2], z_sems, 2, far)
+        forward = joined((d, 0), h)
+        receive(y_s.at[d, :, cols(h)], y_sems, 2 * d + h)
+        forward = forward + y_s[d, :, cols(h)].astype(jnp.float32)
+        if d == 2:
+            receive(z_part(1, h), z_sems, 2 + h)
+            forward = forward + z_s[1, :, cols(h)].astype(jnp.float32)
+        if d:
+            sum_s[here, cols(h)] = forward.astype(jnp.bfloat16)
+            slot_of = d // 2 if d % 2 else 2
+            send(
+                sum_s.at[here, cols(h)],
+                z_part(slot_of, h),
+                z_sems,
+                2 * slot_of + h,
+                close if d % 2 else far,
+            )
+        else:
+            ends.append(forward)
     for i in (0, 2):
-        receive(z_s.at[i], z_sems, i)
-        forward = forward + z_s[i].astype(jnp.float32)
+        for h in (0, 1):
+            receive(z_part(i, h), z_sems, 2 * i + h)
+            ends[h] = ends[h] + z_s[i, :, cols(h)].astype(jnp.float32)
+    forward = jnp.concatenate(ends, axis=1)
     forward = forward.astype(jnp.bfloat16).astype(jnp.float32)
     own_half = pl.ds(pl.multiple_of(t * feat, feat), feat)
     final = residual_scale * mid_s[rows_of(f), own_half].astype(jnp.float32) + forward
@@ -788,9 +813,9 @@
             dma(4 * n_fs),
             dma(9),
             dma(8),
+            dma(2 * n_fs + 1),
+            dma(7),
             dma(n_fs + 1),
-            dma(4),
-            dma(n_fs // 2 + 1),
         ],
         compiler_params=pltpu.CompilerParams(
             collective_id=0, has_side_effects=True, vmem_limit_bytes=60 * 2**20
@@ -833,7 +858,7 @@
         and args[3].shape[0] <= 33
         and lin_weight.shape[1] * 2 == n_fs * LANES
         and conv_out_weight.shape[1] == n_tp * LANES
-        and feat % LANES == 0
+        and feat % (2 * LANES) == 0
         and units % (2 * LANES) == 0
         and narrow == width - LANES > 0
         and lin_weight.shape[0] % 32 == 0

time: 113 us -> 111 us (0.982)
    pallas_call x1, Pallas kernels: 111 us -> 110 us  [by_kernel(): pl.pallas_call(functools.partial(fused, n_fs, n_tp, width, narrow), out_s...]
where the time goes in v4:
time: 111 us
  Pallas kernels  110 us (99%)
  local copies, waits for them, and re-layouts  1.57 us (1%)
    pallas_call x1, Pallas kernels, by_kernel(): pl.pallas_call(functools.partial(fused, n_fs, n_tp, width, narrow), out_s...  110 us

profile of v4, /device:TPU:23, one launch (start us, length us, event | category | flops | bytes accessed | tf_op | source)
XLA Modules:
  0.0 111.3 jit_solution(13807353428837377781)
XLA Ops:
  0.0 109.7 %shard_map.109 = bf16[1,64,1024]{2,1,0:T(8,128)(2,1)} custom-call(bf16[64,1024]{1,0:T(8,128)(2,1)} %bitcast.4, bf16[256,512]{1,0:T(8,128)(2,1)} %lin_hbm.1, bf16[256,512]{1,0:T(8,128)(2,1)} %glu_hbm.1, f32[31,512]{1,0:T(8,128)} %taps_hbm.1, f32[1,512]{1,0:T(1,128)} %bitcast.7, bf16[512,256]{1,0:T(8,128)(2,1)} %out_weight.1, f32[1,2048]{1,0:T(1,128)} %bitcast.5, ...), custom_call_target="tpu_custom_call" | custom-call | tf_op jit(solution)/shard_map/pallas_call | solution.py:775
  109.7 1.6 %copy.13 = bf16[1,64,1024]{2,1,0:T(8,128)(2,1)} copy(bf16[1,64,1024]{2,1,0:T(8,128)(2,1)} %shard_map.109) | data formatting | bytes 262144

commit v5 on v4

--- a/solution.py
+++ b/solution.py
@@ -138,9 +138,9 @@
     "m3": ((0, G, 1, 1),),
     "m4": ((1, D, 1, 0), (0, U, 1, 1),),
     "m5": ((1, D, 2, 1), (1, D, 3, 1), (1, D, 1, 1),),
-    "m6": ((0, D, 2, 0),),
-    "m7": ((0, D, 3, 0),),
+    "m7": ((0, D, 2, 0),),
     "w2": ((0, D, 3, 1), (0, D, 2, 1),),
+    "m8": ((0, D, 3, 0),),
 }
 OUTER = {
     "t3": ((1, G, 2, 0), (1, G, 3, 0),),
@@ -160,9 +160,9 @@
     "m4": ((0, U, 1, 1),),
     "m5": ((1, D, 3, 0), (1, D, 2, 1), (1, D, 3, 1),),
     "m7": ((0, D, 2, 0), (1, D, 1, 0), (1, D, 1, 1),),
-    "m8": ((0, D, 3, 0),),
     "w2": ((0, D, 3, 1), (0, D, 2, 1),),
     "t0": ((1, G, 0, 1),),
+    "e0": ((0, D, 3, 0),),
 }
 
 def fused(

time: 111 us -> 111 us (level)
  no operation moved by 1% of the time
where the time goes in v5:
time: 111 us
  Pallas kernels  110 us (99%)
  local copies, waits for them, and re-layouts  1.57 us (1%)
    pallas_call x1, Pallas kernels, by_kernel(): pl.pallas_call(functools.partial(fused, n_fs, n_tp, width, narrow), out_s...  110 us

profile of v5, /device:TPU:23, one launch (start us, length us, event | category | flops | bytes accessed | tf_op | source)
XLA Modules:
  0.0 111.3 jit_solution(16975982396151492329)
XLA Ops:
  0.0 109.7 %shard_map.109 = bf16[1,64,1024]{2,1,0:T(8,128)(2,1)} custom-call(bf16[64,1024]{1,0:T(8,128)(2,1)} %bitcast.4, bf16[256,512]{1,0:T(8,128)(2,1)} %lin_hbm.1, bf16[256,512]{1,0:T(8,128)(2,1)} %glu_hbm.1, f32[31,512]{1,0:T(8,128)} %taps_hbm.1, f32[1,512]{1,0:T(1,128)} %bitcast.7, bf16[512,256]{1,0:T(8,128)(2,1)} %out_weight.1, f32[1,2048]{1,0:T(1,128)} %bitcast.5, ...), custom_call_target="tpu_custom_call" | custom-call | tf_op jit(solution)/shard_map/pallas_call | solution.py:775
  109.7 1.6 %copy.13 = bf16[1,64,1024]{2,1,0:T(8,128)(2,1)} copy(bf16[1,64,1024]{2,1,0:T(8,128)(2,1)} %shard_map.109) | data formatting | bytes 262144
